TPU v7x, 32 devices: a whole 2x2x4 slice. The times are simulated.
32 devices in a mesh: grp: 2 (over y), sp: 4 (over z), tp: 4 (over x, core).
Axes of the slice: x: 2, y: 2, z: 4, core: 2. Of those that a mesh axis runs over, the one named last changes fastest.
Arguments:
- query_rows: bfloat16 [1024, 1024], P(('grp', 'sp'), 'tp'), parts along dimension 0, may hold values from -12 to 12
- key_rows: bfloat16 [1024, 1024], P(('grp', 'sp'), 'tp'), parts along dimension 0, may hold values from -9 to 9
- value_rows: bfloat16 [1024, 1024], P(('grp', 'sp'), 'tp'), parts along dimension 0, may hold values from -6 to 6
- key_logit: bfloat16 [1024, 8], P(('grp', 'sp'), 'tp'), parts along dimension 0, as said below
- residual: bfloat16 [1024, 2048], P(('grp', 'sp')), parts along dimension 0, may hold values from -6 to 6
- out_weight: bfloat16 [1024, 2048], P('tp'), may hold values from -0.1875 to 0.1875
- mix_gain: float32 [2048], replicated, may hold values from 0.1 to 1.9
- ffn_gain: float32 [2048], replicated, may hold values from 0.1 to 1.9
- out_gain: float32 [2048], replicated, may hold values from 0.1 to 1.9
- gate_weight: bfloat16 [2048, 5120], P('sp', 'tp'), may hold values from -0.125 to 0.125
- up_weight: bfloat16 [2048, 5120], P('sp', 'tp'), may hold values from -0.125 to 0.125
- down_weight: bfloat16 [2048, 5120], P('sp', 'tp'), may hold values from -0.078125 to 0.078125
Outputs:
- layer_out: bfloat16 [1024, 2048], P(('grp', 'sp')), parts along dimension 0
There are 2 independent parts, one for each index of `grp`. A program takes and returns all parts, laid end to end along the dimension named above; an argument that names none is the same for every part. Nothing has to cross between parts.
Inputs may be any that keep to these rules, and one draw needn't show every extreme that they name: `key_logit`: log-odds offsets of the keys, all negative.
All inputs are finite; a program needn't handle non-finite values.
Results may differ from a plain program's by a relative error of at most 0.018.
Values may be sent and summed in bfloat16 or wider, within the bound.
No kernel may reach another device: no remote copies, remote signals or barrier semaphores. Data moves between devices by JAX's collectives and lax.ppermute only.
A program may use at most 64 MiB of HBM per device.

v0:
```python
import functools

import jax
import jax.numpy as jnp
from jax import lax
from jax.experimental import pallas as pl
from jax.experimental.pallas import tpu as pltpu
from jax.sharding import PartitionSpec as P


epsilon = 1e-06
lanes = 128
pad_rows = 16


def normalize(payload_table):
    return payload_table * lax.rsqrt(
        jnp.mean(payload_table * payload_table, axis=-1, keepdims=True) + epsilon
    )


def shift(rows, axis, step):
    count = lax.axis_size(axis)
    return lax.ppermute(rows, axis, [(i, (i + step) % count) for i in range(count)])


def upward(rows, axis, step):
    count = lax.axis_size(axis)
    return lax.ppermute(rows, axis, [(i, i + step) for i in range(count - step)])


def swap(rows, axis, bit):
    count = lax.axis_size(axis)
    return lax.ppermute(rows, axis, [(i, i ^ bit) for i in range(count)])


def call(kernel, outs, flops, *args, scalars=0, scratch=(), limit=None):
    specs = [pl.BlockSpec(memory_space=pltpu.SMEM)] * scalars
    specs += [pl.BlockSpec(memory_space=pltpu.VMEM)] * (len(args) - scalars)
    single = not isinstance(outs, list)
    out_list = [outs] if single else outs
    moved = sum(a.size * a.dtype.itemsize for a in (*args, *out_list))
    out_specs = [pl.BlockSpec(memory_space=pltpu.VMEM)] * len(out_list)
    return pl.pallas_call(
        kernel,
        out_shape=outs,
        in_specs=specs,
        out_specs=out_specs[0] if single else out_specs,
        scratch_shapes=list(scratch),
        compiler_params=pltpu.CompilerParams(vmem_limit_bytes=limit),
        cost_estimate=pl.CostEstimate(flops=flops, bytes_accessed=moved, transcendentals=0),
    )(*args)


def dot_t(a, b):
    return lax.dot_general(a, b, (((1,), (1,)), ((), ())), preferred_element_type=jnp.float32)


def pack_kernel(key_ref, value_ref, logit_ref, out_ref):
    tok_rows, width = key_ref.shape
    out_ref[:tok_rows, :width] = key_ref[...]
    out_ref[:tok_rows, width:] = value_ref[...]
    out_ref[tok_rows:, :tok_rows] = logit_ref[...]
    out_ref[tok_rows:, tok_rows:] = jnp.zeros((pad_rows, 2 * width - tok_rows), out_ref.dtype)


def attend_kernel(head_count, query_ref, *refs):
    blocks, out_ref = refs[:-1], refs[-1]
    tok_rows, width = query_ref.shape
    head_width = width // head_count
    row = lax.broadcasted_iota(jnp.int32, (tok_rows, tok_rows), 0)
    column = lax.broadcasted_iota(jnp.int32, (tok_rows, tok_rows), 1)
    causal = row > column
    later = causal.astype(jnp.float32).astype(jnp.bfloat16)
    for head in range(head_count):
        own = slice(head * head_width, (head + 1) * head_width)
        queries = query_ref[:, own]
        attended = jnp.zeros((tok_rows, head_width), jnp.float32)
        carried = jnp.zeros((tok_rows, 1), jnp.float32)
        for step, block in enumerate(blocks):
            keys = block[:tok_rows, own]
            values = block[:tok_rows, width + head * head_width : width + (head + 1) * head_width]
            logit = block[tok_rows:, :tok_rows].astype(jnp.float32)[head : head + 1]
            scores = dot_t(queries, keys) * head_width ** (-0.5) + logit
            tail = jnp.log(1.0 + jnp.exp(-jnp.abs(scores)))
            keep_log = -jnp.maximum(scores, 0.0) - tail
            take_log = jnp.minimum(scores, 0.0) - tail
            if step == 0:
                keep_log = jnp.where(causal, keep_log, 0.0)
            high = keep_log.astype(jnp.bfloat16)
            rest = keep_log - high.astype(jnp.float32)
            middle = rest.astype(jnp.bfloat16)
            low = (rest - middle.astype(jnp.float32)).astype(jnp.bfloat16)
            within = (
                jnp.dot(high, later, preferred_element_type=jnp.float32)
                + jnp.dot(middle, later, preferred_element_type=jnp.float32)
                + jnp.dot(low, later, preferred_element_type=jnp.float32)
            )
            sticks = jnp.exp(take_log + within)
            if step == 0:
                sticks = jnp.where(causal, sticks, 0.0)
            partial = jnp.dot(
                sticks.astype(jnp.bfloat16), values, preferred_element_type=jnp.float32
            )
            attended = attended + jnp.exp(carried) * partial
            carried = carried + within[:, :1] + keep_log[:, :1]
        out_ref[:, own] = attended.astype(out_ref.dtype)


def attend(queries, key_part, value_part, logit_part):
    tok_rows, width = queries.shape
    head_count = logit_part.shape[1]
    ring = lax.axis_size("sp")
    logit_rows = jnp.pad(jnp.transpose(logit_part), ((0, pad_rows - head_count), (0, 0)))
    packed = call(
        pack_kernel,
        jax.ShapeDtypeStruct((tok_rows + pad_rows, 2 * width), key_part.dtype),
        1,
        key_part,
        value_part,
        logit_rows,
    )
    blocks = [packed] + [upward(packed, "sp", step) for step in range(1, ring)]
    attended = call(
        functools.partial(attend_kernel, head_count),
        jax.ShapeDtypeStruct((tok_rows, width), jnp.bfloat16),
        10 * ring * tok_rows * tok_rows * width,
        queries,
        *blocks,
    )
    return attended, packed


def spread(weight):
    ring, own = lax.axis_size("sp"), lax.axis_index("sp")
    copies, copy = lax.axis_size("grp"), lax.axis_index("grp")
    rows, columns = weight.shape
    part, share = columns // ring, rows // copies
    pieces = weight.reshape(rows, ring, part).transpose(1, 0, 2)
    result = jnp.zeros((ring * rows, part), weight.dtype)
    mine = lax.dynamic_index_in_dim(pieces, own, 0, keepdims=False)
    result = lax.dynamic_update_slice(result, mine, (own * rows, 0))
    for step in range(1, ring):
        target, source = (own + step) % ring, (own - step) % ring
        piece = lax.dynamic_slice(pieces, (target, copy * share, 0), (1, share, part))[0]
        piece = shift(piece, "sp", step)
        for turn in range(copies):
            other = piece if turn == 0 else shift(piece, "grp", turn)
            place = (copy - turn) % copies
            result = lax.dynamic_update_slice(result, other, (source * rows + place * share, 0))
    return result


def tile_at(ref, rows, ring, target):
    main = ref.shape[1] // ring // lanes * lanes
    start = pl.multiple_of(ring * main + target // 2 * lanes, lanes)
    return ref[rows, pl.ds(start, lanes)].astype(jnp.float32)


def main_at(ref, rows, ring, target):
    main = ref.shape[1] // ring // lanes * lanes
    return ref[rows, pl.ds(pl.multiple_of(target * main, lanes), main)]


def halves(low, high, odd):
    lower = lax.broadcasted_iota(jnp.int32, low.shape, 1) < lanes // 2
    low = jnp.where(odd, pltpu.roll(low, lanes // 2, 1), low)
    high = jnp.where(odd, high, pltpu.roll(high, lanes // 2, 1))
    return jnp.where(lower, low, high).astype(jnp.bfloat16)


def pack_wide_kernel(ring, where_ref, gate_ref, up_ref, own_ref, *out_refs):
    own, copy = where_ref[0], where_ref[1]
    share = out_refs[0].shape[0]
    for step in range(ring):
        target = lax.rem(own + step, ring)
        out = own_ref if step == 0 else out_refs[step - 1]
        rows = slice(None) if step == 0 else pl.ds(pl.multiple_of(copy * share, share), share)
        gate, up = main_at(gate_ref, rows, ring, target), main_at(up_ref, rows, ring, target)
        main = gate.shape[1]
        out[:, :main] = gate
        out[:, main : 2 * main] = up
        out[:, 2 * main :] = halves(
            tile_at(gate_ref, rows, ring, target),
            tile_at(up_ref, rows, ring, target),
            target % 2 == 1,
        )


def pack_narrow_kernel(ring, where_ref, down_ref, *out_refs):
    own, copy = where_ref[0], where_ref[1]
    half = out_refs[0].shape[0]
    copies = down_ref.shape[0] // (2 * half)
    for step in range(1 - copies, ring):
        target = lax.rem(own + max(step, 0), ring)
        out = out_refs[step + copies - 1]
        start = (step + copies - 1) * 2 * half if step <= 0 else copy * 2 * half
        upper = pl.ds(pl.multiple_of(start, half), half)
        lower = pl.ds(pl.multiple_of(start + half, half), half)
        main = (out.shape[1] - lanes) // 2
        out[:, :main] = main_at(down_ref, upper, ring, target)
        out[:, main : 2 * main] = main_at(down_ref, lower, ring, target)
        out[:, 2 * main :] = halves(
            tile_at(down_ref, upper, ring, target),
            tile_at(down_ref, lower, ring, target),
            target % 2 == 1,
        )


def exchange(pieces):
    copies = lax.axis_size("grp")
    arrived = []
    for step, piece in enumerate(pieces, 1):
        piece = shift(piece, "sp", step)
        arrived.append([piece] + [shift(piece, "grp", turn) for turn in range(1, copies)])
    return arrived


def wide_kernel(ring, copies, block_count, where_ref, *refs):
    blocks, refs = refs[:block_count], refs[block_count:]
    own_ref, pieces, (low_ref, high_ref), scratch = refs[0], refs[1:-4], refs[-4:-2], refs[-2:]
    weight, rows_ref = scratch
    own, copy = where_ref[0], where_ref[1]
    block_rows = blocks[0].shape[0]
    for index, block in enumerate(blocks):
        rows_ref[index * block_rows : (index + 1) * block_rows, :] = block[...]
    depth, share = own_ref.shape[0], pieces[0].shape[0]
    weight[pl.ds(pl.multiple_of(own * depth, depth), depth), :] = own_ref[...]
    for step in range(1, ring):
        for turn in range(copies):
            source = lax.rem(own - step + ring, ring)
            place = lax.rem(copy - turn + copies, copies)
            start = pl.multiple_of(source * depth + place * share, share)
            weight[pl.ds(start, share), :] = pieces[(step - 1) * copies + turn][...]
    main = (own_ref.shape[1] - lanes) // 2
    count = rows_ref.shape[0]
    tile = min(count, 256)

    def body(index, _):
        rows = pl.ds(pl.multiple_of(index * tile, tile), tile)
        block = rows_ref[rows, :]
        gate = jnp.dot(block, weight[:, :main], preferred_element_type=jnp.float32)
        up = jnp.dot(block, weight[:, main : 2 * main], preferred_element_type=jnp.float32)
        both = jnp.dot(block, weight[:, 2 * main :], preferred_element_type=jnp.float32)
        hidden = (gate / (1.0 + jnp.exp(-gate)) * up).astype(jnp.bfloat16)
        rest = both / (1.0 + jnp.exp(-both)) * pltpu.roll(both, lanes // 2, 1)
        lower = lax.broadcasted_iota(jnp.int32, rest.shape, 1) < lanes // 2
        rest = jnp.where(lower, rest, 0.0)
        low_ref[rows, :main] = hidden
        high_ref[rows, :main] = hidden
        low_ref[rows, main:] = rest.astype(jnp.bfloat16)
        high_ref[rows, main:] = pltpu.roll(rest, lanes // 2, 1).astype(jnp.bfloat16)
        return 0

    lax.fori_loop(0, count // tile, body, 0)


def narrow_kernel(ring, copies, where_ref, low_ref, high_ref, *refs):
    own_refs, pieces, outs, weights = refs[:copies], refs[copies:-4], refs[-4:-2], refs[-2:]
    own, copy = where_ref[0], where_ref[1]
    half = own_refs[0].shape[0]
    main = (own_refs[0].shape[1] - lanes) // 2

    def place_piece(ref, source, place):
        start = pl.multiple_of((source * copies + place) * half, half)
        for part, weight in enumerate(weights):
            weight[pl.ds(start, half), :main] = ref[:, part * main : (part + 1) * main]
            weight[pl.ds(start, half), main:] = ref[:, 2 * main :]

    for place in range(copies):
        place_piece(own_refs[place], own, place)
    for step in range(1, ring):
        for turn in range(copies):
            source = lax.rem(own - step + ring, ring)
            place = lax.rem(copy - turn + copies, copies)
            place_piece(pieces[(step - 1) * copies + turn], source, place)
    count = outs[0].shape[0]
    for index, out in enumerate(outs):
        rows = slice(index * count, (index + 1) * count)
        for part, hidden_ref in enumerate((low_ref, high_ref)):
            units = dot_t(hidden_ref[rows, :], weights[part][...]).astype(jnp.bfloat16)
            for block in range(ring * copies):
                start = (2 * block + part) * half
                out[:, start : start + half] = units[:, block * half : (block + 1) * half]


def join_kernel(member_ref, *refs):
    parts, out_ref = refs[:-1], refs[-1]
    rows = parts[0].shape[0]
    for offset, part in enumerate(parts):
        start = pl.multiple_of((member_ref[0] ^ offset) * rows, rows)
        out_ref[pl.ds(start, rows), :] = part[...]


def shards(
    query_rows,
    key_rows,
    value_rows,
    key_logit,
    residual,
    out_weight,
    mix_gain,
    ffn_gain,
    out_gain,
    gate_weight,
    up_weight,
    down_weight,
):
    ring, own = lax.axis_size("sp"), lax.axis_index("sp")
    copies, copy = lax.axis_size("grp"), lax.axis_index("grp")
    members, member = lax.axis_size("tp"), lax.axis_index("tp")
    tok_rows, width = residual.shape
    own_rows = tok_rows // members
    bits = [1 << i for i in range(members.bit_length() - 1)]
    depth, part = gate_weight.shape[0], gate_weight.shape[1] // ring
    main, share = part // lanes * lanes, depth // copies
    packs = main > 0 and 2 * (part - main) == lanes and ring % 2 == 0 and share % 32 == 0
    where = jnp.stack([own, copy]).astype(jnp.int32)

    attended, packed = attend(query_rows, key_rows, value_rows, key_logit)
    if packs:
        shape = jax.ShapeDtypeStruct
        gate_in, up_in, _ = lax.optimization_barrier((gate_weight, up_weight, packed))
        wide_own, *wide = call(
            functools.partial(pack_wide_kernel, ring),
            [shape((depth, 2 * part), jnp.bfloat16)]
            + [shape((share, 2 * part), jnp.bfloat16)] * (ring - 1),
            1,
            where,
            gate_in,
            up_in,
            scalars=1,
        )
        wide = [piece for group in exchange(wide) for piece in group]

    head_part = jnp.dot(attended, out_weight, preferred_element_type=jnp.float32)
    head_part = head_part.astype(jnp.bfloat16).reshape(members, own_rows, width)
    mixed = jnp.zeros((own_rows, width), jnp.float32)
    for step in range(members):
        piece = lax.dynamic_index_in_dim(head_part, member ^ step, 0, keepdims=False)
        piece = piece if step == 0 else swap(piece, "tp", step)
        mixed = mixed + piece.astype(jnp.float32)
    mixed = mixed.astype(jnp.bfloat16)
    own_residual = lax.dynamic_slice_in_dim(residual, member * own_rows, own_rows, 0)
    middle = (
        own_residual.astype(jnp.float32) + mix_gain * normalize(mixed.astype(jnp.float32))
    ).astype(jnp.bfloat16)
    normed = (ffn_gain * normalize(middle.astype(jnp.float32))).astype(jnp.bfloat16)

    if packs:
        narrow = call(
            functools.partial(pack_narrow_kernel, ring),
            [shape((share // 2, 2 * part), jnp.bfloat16)] * (ring - 1 + copies),
            1,
            where,
            down_weight,
            scalars=1,
        )
        narrow_own, narrow = narrow[:copies], narrow[copies:]
        narrow = [piece for group in exchange(narrow) for piece in group]

        blocks = {(0, 0): normed}
        for step in range(1, ring):
            blocks[0, step] = shift(normed, "sp", step)
        for bit in reversed(bits):
            for (offset, step), block in list(blocks.items()):
                blocks[offset ^ bit, step] = swap(block, "tp", bit)
        order = [(2 * p + half, k) for half in range(2) for p in range(members // 2) for k in range(ring)]
        all_rows = len(order) * own_rows
        hidden = call(
            functools.partial(wide_kernel, ring, copies, len(order)),
            [shape((all_rows, main + lanes), jnp.bfloat16)] * 2,
            4 * all_rows * width * part,
            where,
            *[blocks[key] for key in order],
            wide_own,
            *wide,
            scalars=1,
            scratch=[
                pltpu.VMEM((width, 2 * part), jnp.bfloat16),
                pltpu.VMEM((all_rows, width), jnp.bfloat16),
            ],
            limit=40 << 20,
        )
        kept, sent = call(
            functools.partial(narrow_kernel, ring, copies),
            [shape((all_rows // 2, width), jnp.bfloat16)] * 2,
            2 * all_rows * width * part,
            where,
            *hidden,
            *narrow_own,
            *narrow,
            scalars=1,
            scratch=[pltpu.VMEM((width // 2, main + lanes), jnp.bfloat16)] * 2,
            limit=40 << 20,
        )
        arrived = swap(sent, "tp", 1)
        kept = kept.reshape(members // 2, ring, own_rows, width)
        arrived = arrived.reshape(members // 2, ring, own_rows, width)
        ffn_out = jnp.zeros((own_rows, width), jnp.float32)
        for step in [*range(1, ring), 0]:
            units = kept[:, step].astype(jnp.float32) + arrived[:, step].astype(jnp.float32)
            for bit in bits[1:]:
                moved = swap(units[1::2].astype(jnp.bfloat16), "tp", bit)
                units = units[0::2] + moved.astype(jnp.float32)
            units = units[0]
            if step:
                units = shift(units.astype(jnp.bfloat16), "sp", -step).astype(jnp.float32)
            ffn_out = ffn_out + units
    else:
        gathered = jnp.stack(
            [normed if step == 0 else shift(normed, "sp", step) for step in range(ring)]
        )[None]
        for bit in reversed(bits):
            gathered = jnp.concatenate([gathered, swap(gathered, "tp", bit)], axis=0)
        gathered = gathered.reshape(members * ring * own_rows, width)
        gate_full, up_full, down_full = spread(gate_weight), spread(up_weight), spread(down_weight)
        gate_act = jnp.dot(gathered, gate_full, preferred_element_type=jnp.float32)
        up_act = jnp.dot(gathered, up_full, preferred_element_type=jnp.float32)
        hidden = (jax.nn.silu(gate_act) * up_act).astype(jnp.bfloat16)
        unit_part = lax.dot_general(
            hidden, down_full, (((1,), (1,)), ((), ())), preferred_element_type=jnp.float32
        ).astype(jnp.bfloat16)
        unit_part = unit_part.reshape(members, ring, own_rows, width)
        for bit in bits:
            kept, sent = jnp.split(unit_part, 2, axis=0)
            unit_part = (
                kept.astype(jnp.float32) + swap(sent, "tp", bit).astype(jnp.float32)
            ).astype(jnp.bfloat16)
        ffn_out = unit_part[0, 0].astype(jnp.float32)
        for step in range(1, ring):
            ffn_out = ffn_out + shift(unit_part[0, step], "sp", -step).astype(jnp.float32)
    ffn_out = ffn_out.astype(jnp.bfloat16)
    layer_out = (
        middle.astype(jnp.float32) + out_gain * normalize(ffn_out.astype(jnp.float32))
    ).astype(jnp.bfloat16)
    parts = {0: layer_out}
    for bit in reversed(bits):
        for offset, rows in list(parts.items()):
            parts[offset ^ bit] = swap(rows, "tp", bit)
    return call(
        join_kernel,
        jax.ShapeDtypeStruct((tok_rows, width), jnp.bfloat16),
        1,
        member[None].astype(jnp.int32),
        *[parts[offset] for offset in range(members)],
        scalars=1,
    )


def solution(mesh):
    placed = (
        P(("grp", "sp"), "tp"),
        P(("grp", "sp"), "tp"),
        P(("grp", "sp"), "tp"),
        P(("grp", "sp"), "tp"),
        P(("grp", "sp"), None),
        P("tp", None),
        P(),
        P(),
        P(),
        P("sp", "tp"),
        P("sp", "tp"),
        P("sp", "tp"),
    )
    return jax.shard_map(
        shards, mesh=mesh, in_specs=placed, out_specs=P(("grp", "sp"), None), check_vma=False
    )
```

profile of v0, /device:TPU:0, one launch (start us, length us, event | category | flops | bytes accessed | tf_op | source)
XLA Modules:
  0.0 162.3 jit_solution(3235809050702139961)
XLA Ops:
  0.0 1.3 pad.4.logit_ref
  1.3 1.5 shard_map.118.refs_0_
  2.9 5.0 %collective-permute-start = (bf16[144,512]{1,0:T(8,128)(2,1)}, bf16[144,512]{1,0:T(8,128)(2,1)S(1)}, u32[]{:S(2)}, u32[]{:S(2)}) collective-permute-start(bf16[144,512]{1,0:T(8,128)(2,1)} %shard_map.118.refs_0_), channel_id=1, source_target_pairs={{0,4},{4,8},{8,12},{1,5},{5,9},{9,13},{2,6},{6,10},{10,14},{3,7},{... | collective-permute-start | bytes 442376 | tf_op jit(solution)/shard_map/ppermute | solution.py:29
  7.8 4.5 %collective-permute-start.1 = (bf16[144,512]{1,0:T(8,128)(2,1)}, bf16[144,512]{1,0:T(8,128)(2,1)S(1)}, u32[]{:S(2)}, u32[]{:S(2)}) collective-permute-start(bf16[144,512]{1,0:T(8,128)(2,1)} %shard_map.118.refs_0_), channel_id=1, source_target_pairs={{0,8},{4,12},{1,9},{5,13},{2,10},{6,14},{3,11},{7,15},{16,24},{20,... | collective-permute-start | bytes 442376 | tf_op jit(solution)/shard_map/ppermute | solution.py:29
  12.3 1.3 collective-permute-start.2
  13.7 3.2 %collective-permute-done.1.refs_2_ = bf16[144,512]{1,0:T(8,128)(2,1)S(1)} collective-permute-done((bf16[144,512]{1,0:T(8,128)(2,1)}, bf16[144,512]{1,0:T(8,128)(2,1)S(1)}, u32[]{:S(2)}, u32[]{:S(2)}) %collective-permute-start.1) | collective-permute-done | bytes 147488 | tf_op jit(solution)/shard_map/ppermute | solution.py:29
  16.9 1.8 %collective-permute-done.2.refs_3_ = bf16[144,512]{1,0:T(8,128)(2,1)S(1)} collective-permute-done((bf16[144,512]{1,0:T(8,128)(2,1)}, bf16[144,512]{1,0:T(8,128)(2,1)S(1)}, u32[]{:S(2)}, u32[]{:S(2)}) %collective-permute-start.2) | collective-permute-done | bytes 147488 | tf_op jit(solution)/shard_map/ppermute | solution.py:29
  19.3 4.1 %shard_map.119 = bf16[128,256]{1,0:T(8,128)(2,1)} custom-call(bf16[128,256]{1,0:T(8,128)(2,1)} %query_ref.1, bf16[144,512]{1,0:T(8,128)(2,1)} %shard_map.118.refs_0_, bf16[144,512]{1,0:T(8,128)(2,1)} %copy-done.6, bf16[144,512]{1,0:T(8,128)(2,1)} %copy-done.7, bf16[144,512]{1,0:T(8,128)(2,1)} %copy-done.8), custom_call_target="tpu_custom_call" | custom-call | flops 167772160 | bytes 720896 | tf_op jit(solution)/shard_map/pallas_call | solution.py:44
  25.3 1.5 collective-permute-start.4
  27.8 3.1 %shard_map.120 = (bf16[512,640]{1,0:T(8,128)(2,1)}, bf16[256,640]{1,0:T(8,128)(2,1)}, bf16[256,640]{1,0:T(8,128)(2,1)}, bf16[256,640]{1,0:T(8,128)(2,1)}) custom-call(s32[2]{0:T(128)} %pad_add_fusion.where_ref, bf16[512,1280]{1,0:T(8,128)(2,1)} %gate_ref, bf16[512,1280]{1,0:T(8,128)(2,1)} %up_ref), custom_call_target="tpu_custom_call" | custom-call | flops 1 | bytes 4259848 | tf_op jit(solution)/shard_map/pallas_call | solution.py:44
  30.9 4.3 %collective-permute-start.21 = (bf16[256,640]{1,0:T(8,128)(2,1)}, bf16[256,640]{1,0:T(8,128)(2,1)S(1)}, u32[]{:S(2)}, u32[]{:S(2)}) collective-permute-start(bf16[256,640]{1,0:T(8,128)(2,1)} %get-tuple-element.23), channel_id=1, source_target_pairs={{0,4},{4,8},{8,12},{12,0},{1,5},{5,9},{9,13},{13,1},{2,6},{6,10},{... | collective-permute-start | bytes 983048 | tf_op jit(solution)/shard_map/ppermute | solution.py:24
  35.2 3.3 %collective-permute-start.23 = (bf16[256,640]{1,0:T(8,128)(2,1)}, bf16[256,640]{1,0:T(8,128)(2,1)S(1)}, u32[]{:S(2)}, u32[]{:S(2)}) collective-permute-start(bf16[256,640]{1,0:T(8,128)(2,1)} %get-tuple-element.24), channel_id=1, source_target_pairs={{0,8},{4,12},{8,0},{12,4},{1,9},{5,13},{9,1},{13,5},{2,10},{6,14},... | collective-permute-start | bytes 983048 | tf_op jit(solution)/shard_map/ppermute | solution.py:24
  38.5 2.4 %shard_map.122 = (bf16[128,640]{1,0:T(8,128)(2,1)}, bf16[128,640]{1,0:T(8,128)(2,1)}, bf16[128,640]{1,0:T(8,128)(2,1)}, bf16[128,640]{1,0:T(8,128)(2,1)}, bf16[128,640]{1,0:T(8,128)(2,1)}) custom-call(s32[2]{0:T(128)} %pad_add_fusion.where_ref, bf16[512,1280]{1,0:T(8,128)(2,1)} %down_ref.1), custom_call_target="tpu_custom_call" | custom-call | flops 1 | bytes 2129928 | tf_op jit(solution)/shard_map/pallas_call | solution.py:44
  40.9 2.0 %collective-permute-start.27 = (bf16[128,640]{1,0:T(8,128)(2,1)}, bf16[128,640]{1,0:T(8,128)(2,1)S(1)}, u32[]{:S(2)}, u32[]{:S(2)}) collective-permute-start(bf16[128,640]{1,0:T(8,128)(2,1)} %get-tuple-element.30), channel_id=1, source_target_pairs={{0,4},{4,8},{8,12},{12,0},{1,5},{5,9},{9,13},{13,1},{2,6},{6,10},{... | collective-permute-start | bytes 491528 | tf_op jit(solution)/shard_map/ppermute | solution.py:24
  43.2 1.2 fusion.6
  44.3 20.1 %collective-permute-done.27.refs_2_ = bf16[128,640]{1,0:T(8,128)(2,1)S(1)} collective-permute-done((bf16[128,640]{1,0:T(8,128)(2,1)}, bf16[128,640]{1,0:T(8,128)(2,1)S(1)}, u32[]{:S(2)}, u32[]{:S(2)}) %collective-permute-start.27) | collective-permute-done | bytes 163872 | tf_op jit(solution)/shard_map/ppermute | solution.py:24
  65.2 12.8 %collective-permute-done.29.refs_4_ = bf16[128,640]{1,0:T(8,128)(2,1)S(1)} collective-permute-done((bf16[128,640]{1,0:T(8,128)(2,1)}, bf16[128,640]{1,0:T(8,128)(2,1)S(1)}, u32[]{:S(2)}, u32[]{:S(2)}) %collective-permute-start.29) | collective-permute-done | bytes 163872 | tf_op jit(solution)/shard_map/ppermute | solution.py:24
  78.3 3.1 %collective-permute-done.31.refs_6_ = bf16[128,640]{1,0:T(8,128)(2,1)S(1)} collective-permute-done((bf16[128,640]{1,0:T(8,128)(2,1)}, bf16[128,640]{1,0:T(8,128)(2,1)S(1)}, u32[]{:S(2)}, u32[]{:S(2)}) %collective-permute-start.31) | collective-permute-done | bytes 163872 | tf_op jit(solution)/shard_map/ppermute | solution.py:24
  81.4 1.2 collective-permute-start.7
  82.7 1.8 %collective-permute-start.8 = (bf16[32,2048]{1,0:T(8,128)(2,1)S(1)}, bf16[32,2048]{1,0:T(8,128)(2,1)S(1)}, u32[]{:S(2)}, u32[]{:S(2)}) collective-permute-start(bf16[32,2048]{1,0:T(8,128)(2,1)S(1)} %fusion.8.refs_0_), channel_id=1, source_target_pairs={{0,12},{4,0},{8,4},{12,8},{1,13},{5,1},{9,5},{13,9},{2,14},{6,2},{... | collective-permute-start | bytes 393224 | tf_op jit(solution)/shard_map/ppermute | solution.py:24
  84.4 1.5 collective-permute-start.9
  86.3 1.5 collective-permute-start.10
  87.8 3.2 %collective-permute-done.7.refs_2_ = bf16[32,2048]{1,0:T(8,128)(2,1)S(1)} collective-permute-done((bf16[32,2048]{1,0:T(8,128)(2,1)S(1)}, bf16[32,2048]{1,0:T(8,128)(2,1)S(1)}, u32[]{:S(2)}, u32[]{:S(2)}) %collective-permute-start.7) | collective-permute-done | bytes 131104 | tf_op jit(solution)/shard_map/ppermute | solution.py:24
  90.9 1.5 collective-permute-start.11
  93.0 1.5 collective-permute-start.22
  95.0 2.3 %collective-permute-done.11.refs_6_ = bf16[32,2048]{1,0:T(8,128)(2,1)S(1)} collective-permute-done((bf16[32,2048]{1,0:T(8,128)(2,1)S(1)}, bf16[32,2048]{1,0:T(8,128)(2,1)S(1)}, u32[]{:S(2)}, u32[]{:S(2)}) %collective-permute-start.11) | collective-permute-done | bytes 131104 | tf_op jit(solution)/shard_map/ppermute | solution.py:34
  97.3 1.5 collective-permute-start.24
  99.1 1.5 collective-permute-start.26
  103.6 7.0 %collective-permute-done.24.refs_20_ = bf16[256,640]{1,0:T(8,128)(2,1)S(1)} collective-permute-done((bf16[256,640]{1,0:T(8,128)(2,1)S(1)}, bf16[256,640]{1,0:T(8,128)(2,1)S(1)}, u32[]{:S(2)}, u32[]{:S(2)}) %collective-permute-start.24) | collective-permute-done | bytes 327712 | tf_op jit(solution)/shard_map/ppermute | solution.py:24
  110.6 1.5 collective-permute-start.28
  112.1 5.5 %collective-permute-done.26.refs_22_ = bf16[256,640]{1,0:T(8,128)(2,1)S(1)} collective-permute-done((bf16[256,640]{1,0:T(8,128)(2,1)S(1)}, bf16[256,640]{1,0:T(8,128)(2,1)S(1)}, u32[]{:S(2)}, u32[]{:S(2)}) %collective-permute-start.26) | collective-permute-done | bytes 327712 | tf_op jit(solution)/shard_map/ppermute | solution.py:24
  117.6 1.5 collective-permute-start.30
  119.7 3.1 %shard_map.121 = (bf16[512,384]{1,0:T(8,128)(2,1)S(1)}, bf16[512,384]{1,0:T(8,128)(2,1)S(1)}) custom-call(s32[2]{0:T(128)S(1)} %copy-done.1, bf16[32,2048]{1,0:T(8,128)(2,1)S(1)} %fusion.8.refs_0_, bf16[32,2048]{1,0:T(8,128)(2,1)S(1)} %collective-permute-done.6.refs_1_, bf16[32,2048]{1,0:T(8,128)(2,1)S(1)} %collective-permute-done.7.refs_2_, ...), custom_call_target="tpu_custom_call" | custom-call | flops 1342177280 | bytes 5505032 | tf_op jit(solution)/shard_map/pallas_call | solution.py:44
  122.8 1.8 %collective-permute-done.30.refs_5_ = bf16[128,640]{1,0:T(8,128)(2,1)S(1)} collective-permute-done((bf16[128,640]{1,0:T(8,128)(2,1)S(1)}, bf16[128,640]{1,0:T(8,128)(2,1)S(1)}, u32[]{:S(2)}, u32[]{:S(2)}) %collective-permute-start.30) | collective-permute-done | bytes 163872 | tf_op jit(solution)/shard_map/ppermute | solution.py:24
  124.7 1.9 %collective-permute-done.32.refs_7_ = bf16[128,640]{1,0:T(8,128)(2,1)S(1)} collective-permute-done((bf16[128,640]{1,0:T(8,128)(2,1)S(1)}, bf16[128,640]{1,0:T(8,128)(2,1)S(1)}, u32[]{:S(2)}, u32[]{:S(2)}) %collective-permute-start.32) | collective-permute-done | bytes 163872 | tf_op jit(solution)/shard_map/ppermute | solution.py:24
  126.5 1.9 %shard_map.123 = (bf16[256,2048]{1,0:T(8,128)(2,1)S(1)}, bf16[256,2048]{1,0:T(8,128)(2,1)S(1)}) custom-call(s32[2]{0:T(128)S(1)} %copy-done.1, bf16[512,384]{1,0:T(8,128)(2,1)S(1)} %get-tuple-element.26.low_ref, bf16[512,384]{1,0:T(8,128)(2,1)S(1)} %get-tuple-element.27.high_ref, bf16[128,640]{1,0:T(8,128)(2,1)S(1)} %copy-done.3, ...), custom_call_target="tpu_custom_call" | custom-call | flops 671088640 | bytes 4194312 | tf_op jit(solution)/shard_map/pallas_call | solution.py:44
  128.6 2.6 %collective-permute-done.33 = bf16[256,2048]{1,0:T(8,128)(2,1)S(1)} collective-permute-done((bf16[256,2048]{1,0:T(8,128)(2,1)S(1)}, bf16[256,2048]{1,0:T(8,128)(2,1)S(1)}, u32[]{:S(2)}, u32[]{:S(2)}) %collective-permute-start.33) | collective-permute-done | bytes 1048608 | tf_op jit(solution)/shard_map/ppermute | solution.py:34
  131.6 1.6 collective-permute-start.34
  133.8 1.6 collective-permute-start.38
  136.0 2.0 %collective-permute-done.34 = bf16[1,32,2048]{2,1,0:T(8,128)(2,1)S(1)} collective-permute-done((bf16[1,32,2048]{2,1,0:T(8,128)(2,1)S(1)}, bf16[1,32,2048]{2,1,0:T(8,128)(2,1)S(1)}, u32[]{:S(2)}, u32[]{:S(2)}) %collective-permute-start.34) | collective-permute-done | bytes 131104 | tf_op jit(solution)/shard_map/ppermute | solution.py:34
  138.1 1.7 %collective-permute-start.35 = (bf16[32,2048]{1,0:T(8,128)(2,1)S(1)}, bf16[32,2048]{1,0:T(8,128)(2,1)S(1)}, u32[]{:S(2)}, u32[]{:S(2)}) collective-permute-start(bf16[32,2048]{1,0:T(8,128)(2,1)S(1)} %fusion.23), channel_id=1, source_target_pairs={{0,12},{4,0},{8,4},{12,8},{1,13},{5,1},{9,5},{13,9},{2,14},{6,2},{... | collective-permute-start | bytes 393224 | tf_op jit(solution)/shard_map/ppermute | solution.py:24
  140.9 2.2 %collective-permute-start.37 = (bf16[32,2048]{1,0:T(8,128)(2,1)S(1)}, bf16[32,2048]{1,0:T(8,128)(2,1)S(1)}, u32[]{:S(2)}, u32[]{:S(2)}) collective-permute-start(bf16[32,2048]{1,0:T(8,128)(2,1)S(1)} %fusion.25), channel_id=1, source_target_pairs={{0,8},{4,12},{8,0},{12,4},{1,9},{5,13},{9,1},{13,5},{2,10},{6,14},... | collective-permute-start | bytes 393224 | tf_op jit(solution)/shard_map/ppermute | solution.py:24
  143.7 3.2 %collective-permute-start.39 = (bf16[32,2048]{1,0:T(8,128)(2,1)S(1)}, bf16[32,2048]{1,0:T(8,128)(2,1)S(1)}, u32[]{:S(2)}, u32[]{:S(2)}) collective-permute-start(bf16[32,2048]{1,0:T(8,128)(2,1)S(1)} %fusion.27), channel_id=1, source_target_pairs={{0,4},{4,8},{8,12},{12,0},{1,5},{5,9},{9,13},{13,1},{2,6},{6,10},{... | collective-permute-start | bytes 393224 | tf_op jit(solution)/shard_map/ppermute | solution.py:24
  146.8 6.1 %collective-permute-done.37 = bf16[32,2048]{1,0:T(8,128)(2,1)S(1)} collective-permute-done((bf16[32,2048]{1,0:T(8,128)(2,1)S(1)}, bf16[32,2048]{1,0:T(8,128)(2,1)S(1)}, u32[]{:S(2)}, u32[]{:S(2)}) %collective-permute-start.37) | collective-permute-done | bytes 131104 | tf_op jit(solution)/shard_map/ppermute | solution.py:24
  153.3 1.3 collective-permute-start.42
  154.6 3.8 %collective-permute-done.42.refs_2_ = bf16[32,2048]{1,0:T(8,128)(2,1)S(1)} collective-permute-done((bf16[32,2048]{1,0:T(8,128)(2,1)S(1)}, bf16[32,2048]{1,0:T(8,128)(2,1)S(1)}, u32[]{:S(2)}, u32[]{:S(2)}) %collective-permute-start.42) | collective-permute-done | bytes 131104 | tf_op jit(solution)/shard_map/ppermute | solution.py:34
  158.4 1.3 collective-permute-done.43.refs_3_
  160.4 1.9 %shard_map.124 = bf16[128,2048]{1,0:T(8,128)(2,1)} custom-call(s32[1]{0:T(128)} %bitcast.member_ref, bf16[32,2048]{1,0:T(8,128)(2,1)} %copy-done.5, bf16[32,2048]{1,0:T(8,128)(2,1)} %copy-done.10, bf16[32,2048]{1,0:T(8,128)(2,1)} %copy-done.9, bf16[32,2048]{1,0:T(8,128)(2,1)} %copy-done.11), custom_call_target="tpu_custom_call" | custom-call | flops 1 | bytes 1048580 | tf_op jit(solution)/shard_map/pallas_call | solution.py:44
  (95 shorter events, 14.6 us)
Async XLA Ops:
  0.0 23.4 %copy-start = (bf16[256,2048]{1,0:T(8,128)(2,1)S(1)}, bf16[256,2048]{1,0:T(8,128)(2,1)}, u32[]{:S(2)}) copy-start(bf16[256,2048]{1,0:T(8,128)(2,1)} %param.17) | copy-start | bytes 3145732
  2.9 10.8 %collective-permute-start = (bf16[144,512]{1,0:T(8,128)(2,1)}, bf16[144,512]{1,0:T(8,128)(2,1)S(1)}, u32[]{:S(2)}, u32[]{:S(2)}) collective-permute-start(bf16[144,512]{1,0:T(8,128)(2,1)} %shard_map.118.refs_0_), channel_id=1, source_target_pairs={{0,4},{4,8},{8,12},{1,5},{5,9},{9,13},{2,6},{6,10},{10,14},{3,7},{... | collective-permute-start | bytes 442376 | tf_op jit(solution)/shard_map/ppermute | solution.py:29
  7.8 9.0 %collective-permute-start.1 = (bf16[144,512]{1,0:T(8,128)(2,1)}, bf16[144,512]{1,0:T(8,128)(2,1)S(1)}, u32[]{:S(2)}, u32[]{:S(2)}) collective-permute-start(bf16[144,512]{1,0:T(8,128)(2,1)} %shard_map.118.refs_0_), channel_id=1, source_target_pairs={{0,8},{4,12},{1,9},{5,13},{2,10},{6,14},{3,11},{7,15},{16,24},{20,... | collective-permute-start | bytes 442376 | tf_op jit(solution)/shard_map/ppermute | solution.py:29
  12.3 6.3 %collective-permute-start.2 = (bf16[144,512]{1,0:T(8,128)(2,1)}, bf16[144,512]{1,0:T(8,128)(2,1)S(1)}, u32[]{:S(2)}, u32[]{:S(2)}) collective-permute-start(bf16[144,512]{1,0:T(8,128)(2,1)} %shard_map.118.refs_0_), channel_id=1, source_target_pairs={{0,12},{1,13},{2,14},{3,15},{16,28},{17,29},{18,30},{19,31}} | collective-permute-start | bytes 442376 | tf_op jit(solution)/shard_map/ppermute | solution.py:29
  25.3 15.6 %collective-permute-start.3 = (bf16[32,2048]{1,0:T(8,128)(2,1)}, bf16[32,2048]{1,0:T(8,128)(2,1)S(1)}, u32[]{:S(2)}, u32[]{:S(2)}) collective-permute-start(bf16[32,2048]{1,0:T(8,128)(2,1)} %get-tuple-element.45), channel_id=1, source_target_pairs={{0,1},{1,0},{2,3},{3,2},{4,5},{5,4},{6,7},{7,6},{8,9},{9,8},{10,11... | collective-permute-start | bytes 393224 | tf_op jit(solution)/shard_map/ppermute | solution.py:34
  25.3 15.6 %collective-permute-start.4 = (bf16[32,2048]{1,0:T(8,128)(2,1)S(1)}, bf16[32,2048]{1,0:T(8,128)(2,1)S(1)}, u32[]{:S(2)}, u32[]{:S(2)}) collective-permute-start(bf16[32,2048]{1,0:T(8,128)(2,1)S(1)} %get-tuple-element.47), channel_id=1, source_target_pairs={{0,2},{1,3},{2,0},{3,1},{4,6},{5,7},{6,4},{7,5},{8,10},{9,11},{10,... | collective-permute-start | bytes 393224 | tf_op jit(solution)/shard_map/ppermute | solution.py:34
  26.8 16.1 %collective-permute-start.5 = (bf16[32,2048]{1,0:T(8,128)(2,1)S(1)}, bf16[32,2048]{1,0:T(8,128)(2,1)S(1)}, u32[]{:S(2)}, u32[]{:S(2)}) collective-permute-start(bf16[32,2048]{1,0:T(8,128)(2,1)S(1)} %get-tuple-element.46), channel_id=1, source_target_pairs={{0,3},{1,2},{2,1},{3,0},{4,7},{5,6},{6,5},{7,4},{8,11},{9,10},{10,... | collective-permute-start | bytes 393224 | tf_op jit(solution)/shard_map/ppermute | solution.py:34
  30.9 51.7 %collective-permute-start.21 = (bf16[256,640]{1,0:T(8,128)(2,1)}, bf16[256,640]{1,0:T(8,128)(2,1)S(1)}, u32[]{:S(2)}, u32[]{:S(2)}) collective-permute-start(bf16[256,640]{1,0:T(8,128)(2,1)} %get-tuple-element.23), channel_id=1, source_target_pairs={{0,4},{4,8},{8,12},{12,0},{1,5},{5,9},{9,13},{13,1},{2,6},{6,10},{... | collective-permute-start | bytes 983048 | tf_op jit(solution)/shard_map/ppermute | solution.py:24
  35.2 84.4 %copy-start.1 = (s32[2]{0:T(128)S(1)}, s32[2]{0:T(128)}, u32[]{:S(2)}) copy-start(s32[2]{0:T(128)} %pad_add_fusion.where_ref) | copy-start | bytes 28
  35.2 84.4 %copy-start.2 = (bf16[512,640]{1,0:T(8,128)(2,1)S(1)}, bf16[512,640]{1,0:T(8,128)(2,1)}, u32[]{:S(2)}) copy-start(bf16[512,640]{1,0:T(8,128)(2,1)} %get-tuple-element.22.refs_16_) | copy-start | bytes 1966084
  35.2 49.2 %collective-permute-start.23 = (bf16[256,640]{1,0:T(8,128)(2,1)}, bf16[256,640]{1,0:T(8,128)(2,1)S(1)}, u32[]{:S(2)}, u32[]{:S(2)}) collective-permute-start(bf16[256,640]{1,0:T(8,128)(2,1)} %get-tuple-element.24), channel_id=1, source_target_pairs={{0,8},{4,12},{8,0},{12,4},{1,9},{5,13},{9,1},{13,5},{2,10},{6,14},... | collective-permute-start | bytes 983048 | tf_op jit(solution)/shard_map/ppermute | solution.py:24
  40.9 45.1 %collective-permute-start.25 = (bf16[256,640]{1,0:T(8,128)(2,1)}, bf16[256,640]{1,0:T(8,128)(2,1)S(1)}, u32[]{:S(2)}, u32[]{:S(2)}) collective-permute-start(bf16[256,640]{1,0:T(8,128)(2,1)} %get-tuple-element.25), channel_id=1, source_target_pairs={{0,12},{4,0},{8,4},{12,8},{1,13},{5,1},{9,5},{13,9},{2,14},{6,2},{... | collective-permute-start | bytes 983048 | tf_op jit(solution)/shard_map/ppermute | solution.py:24
  40.9 23.6 %collective-permute-start.27 = (bf16[128,640]{1,0:T(8,128)(2,1)}, bf16[128,640]{1,0:T(8,128)(2,1)S(1)}, u32[]{:S(2)}, u32[]{:S(2)}) collective-permute-start(bf16[128,640]{1,0:T(8,128)(2,1)} %get-tuple-element.30), channel_id=1, source_target_pairs={{0,4},{4,8},{8,12},{12,0},{1,5},{5,9},{9,13},{13,1},{2,6},{6,10},{... | collective-permute-start | bytes 491528 | tf_op jit(solution)/shard_map/ppermute | solution.py:24
  42.9 35.2 %collective-permute-start.29 = (bf16[128,640]{1,0:T(8,128)(2,1)}, bf16[128,640]{1,0:T(8,128)(2,1)S(1)}, u32[]{:S(2)}, u32[]{:S(2)}) collective-permute-start(bf16[128,640]{1,0:T(8,128)(2,1)} %get-tuple-element.31), channel_id=1, source_target_pairs={{0,8},{4,12},{8,0},{12,4},{1,9},{5,13},{9,1},{13,5},{2,10},{6,14},... | collective-permute-start | bytes 491528 | tf_op jit(solution)/shard_map/ppermute | solution.py:24
  64.4 17.0 %collective-permute-start.31 = (bf16[128,640]{1,0:T(8,128)(2,1)}, bf16[128,640]{1,0:T(8,128)(2,1)S(1)}, u32[]{:S(2)}, u32[]{:S(2)}) collective-permute-start(bf16[128,640]{1,0:T(8,128)(2,1)} %get-tuple-element.32), channel_id=1, source_target_pairs={{0,12},{4,0},{8,4},{12,8},{1,13},{5,1},{9,5},{13,9},{2,14},{6,2},{... | collective-permute-start | bytes 491528 | tf_op jit(solution)/shard_map/ppermute | solution.py:24
  78.0 8.2 %collective-permute-start.6 = (bf16[32,2048]{1,0:T(8,128)(2,1)S(1)}, bf16[32,2048]{1,0:T(8,128)(2,1)S(1)}, u32[]{:S(2)}, u32[]{:S(2)}) collective-permute-start(bf16[32,2048]{1,0:T(8,128)(2,1)S(1)} %fusion.8.refs_0_), channel_id=1, source_target_pairs={{0,4},{4,8},{8,12},{12,0},{1,5},{5,9},{9,13},{13,1},{2,6},{6,10},{... | collective-permute-start | bytes 393224 | tf_op jit(solution)/shard_map/ppermute | solution.py:24
  81.4 9.5 %collective-permute-start.7 = (bf16[32,2048]{1,0:T(8,128)(2,1)S(1)}, bf16[32,2048]{1,0:T(8,128)(2,1)S(1)}, u32[]{:S(2)}, u32[]{:S(2)}) collective-permute-start(bf16[32,2048]{1,0:T(8,128)(2,1)S(1)} %fusion.8.refs_0_), channel_id=1, source_target_pairs={{0,8},{4,12},{8,0},{12,4},{1,9},{5,13},{9,1},{13,5},{2,10},{6,14},... | collective-permute-start | bytes 393224 | tf_op jit(solution)/shard_map/ppermute | solution.py:24
  82.7 9.8 %collective-permute-start.8 = (bf16[32,2048]{1,0:T(8,128)(2,1)S(1)}, bf16[32,2048]{1,0:T(8,128)(2,1)S(1)}, u32[]{:S(2)}, u32[]{:S(2)}) collective-permute-start(bf16[32,2048]{1,0:T(8,128)(2,1)S(1)} %fusion.8.refs_0_), channel_id=1, source_target_pairs={{0,12},{4,0},{8,4},{12,8},{1,13},{5,1},{9,5},{13,9},{2,14},{6,2},{... | collective-permute-start | bytes 393224 | tf_op jit(solution)/shard_map/ppermute | solution.py:24
  84.4 8.5 %collective-permute-start.9 = (bf16[32,2048]{1,0:T(8,128)(2,1)S(1)}, bf16[32,2048]{1,0:T(8,128)(2,1)S(1)}, u32[]{:S(2)}, u32[]{:S(2)}) collective-permute-start(bf16[32,2048]{1,0:T(8,128)(2,1)S(1)} %fusion.8.refs_0_), channel_id=1, source_target_pairs={{0,2},{1,3},{2,0},{3,1},{4,6},{5,7},{6,4},{7,5},{8,10},{9,11},{10,... | collective-permute-start | bytes 393224 | tf_op jit(solution)/shard_map/ppermute | solution.py:34
  85.9 8.6 %collective-permute-start.13 = (bf16[32,2048]{1,0:T(8,128)(2,1)S(1)}, bf16[32,2048]{1,0:T(8,128)(2,1)S(1)}, u32[]{:S(2)}, u32[]{:S(2)}) collective-permute-start(bf16[32,2048]{1,0:T(8,128)(2,1)S(1)} %fusion.8.refs_0_), channel_id=1, source_target_pairs={{0,1},{1,0},{2,3},{3,2},{4,5},{5,4},{6,7},{7,6},{8,9},{9,8},{10,11... | collective-permute-start | bytes 393224 | tf_op jit(solution)/shard_map/ppermute | solution.py:34
  86.3 8.2 %collective-permute-start.10 = (bf16[32,2048]{1,0:T(8,128)(2,1)S(1)}, bf16[32,2048]{1,0:T(8,128)(2,1)S(1)}, u32[]{:S(2)}, u32[]{:S(2)}) collective-permute-start(bf16[32,2048]{1,0:T(8,128)(2,1)S(1)} %collective-permute-done.6.refs_1_), channel_id=1, source_target_pairs={{0,2},{1,3},{2,0},{3,1},{4,6},{5,7},{6,4},{7,5},{8,10},{9,11},{10,... | collective-permute-start | bytes 393224 | tf_op jit(solution)/shard_map/ppermute | solution.py:34
  90.9 6.4 %collective-permute-start.11 = (bf16[32,2048]{1,0:T(8,128)(2,1)S(1)}, bf16[32,2048]{1,0:T(8,128)(2,1)S(1)}, u32[]{:S(2)}, u32[]{:S(2)}) collective-permute-start(bf16[32,2048]{1,0:T(8,128)(2,1)S(1)} %collective-permute-done.7.refs_2_), channel_id=1, source_target_pairs={{0,2},{1,3},{2,0},{3,1},{4,6},{5,7},{6,4},{7,5},{8,10},{9,11},{10,... | collective-permute-start | bytes 393224 | tf_op jit(solution)/shard_map/ppermute | solution.py:34
  92.4 6.7 %collective-permute-start.12 = (bf16[32,2048]{1,0:T(8,128)(2,1)S(1)}, bf16[32,2048]{1,0:T(8,128)(2,1)S(1)}, u32[]{:S(2)}, u32[]{:S(2)}) collective-permute-start(bf16[32,2048]{1,0:T(8,128)(2,1)S(1)} %collective-permute-done.8.refs_3_), channel_id=1, source_target_pairs={{0,2},{1,3},{2,0},{3,1},{4,6},{5,7},{6,4},{7,5},{8,10},{9,11},{10,... | collective-permute-start | bytes 393224 | tf_op jit(solution)/shard_map/ppermute | solution.py:34
  93.0 10.6 %collective-permute-start.22 = (bf16[256,640]{1,0:T(8,128)(2,1)S(1)}, bf16[256,640]{1,0:T(8,128)(2,1)S(1)}, u32[]{:S(2)}, u32[]{:S(2)}) collective-permute-start(bf16[256,640]{1,0:T(8,128)(2,1)S(1)} %collective-permute-done.21.refs_17_), channel_id=1, source_target_pairs={{0,16},{16,0},{1,17},{17,1},{2,18},{18,2},{3,19},{19,3},{4,20},{20... | collective-permute-start | bytes 983048 | tf_op jit(solution)/shard_map/ppermute | solution.py:24
  94.5 6.1 %collective-permute-start.14 = (bf16[32,2048]{1,0:T(8,128)(2,1)S(1)}, bf16[32,2048]{1,0:T(8,128)(2,1)S(1)}, u32[]{:S(2)}, u32[]{:S(2)}) collective-permute-start(bf16[32,2048]{1,0:T(8,128)(2,1)S(1)} %collective-permute-done.6.refs_1_), channel_id=1, source_target_pairs={{0,1},{1,0},{2,3},{3,2},{4,5},{5,4},{6,7},{7,6},{8,9},{9,8},{10,11... | collective-permute-start | bytes 393224 | tf_op jit(solution)/shard_map/ppermute | solution.py:34
  94.5 6.1 %collective-permute-start.15 = (bf16[32,2048]{1,0:T(8,128)(2,1)S(1)}, bf16[32,2048]{1,0:T(8,128)(2,1)S(1)}, u32[]{:S(2)}, u32[]{:S(2)}) collective-permute-start(bf16[32,2048]{1,0:T(8,128)(2,1)S(1)} %collective-permute-done.7.refs_2_), channel_id=1, source_target_pairs={{0,1},{1,0},{2,3},{3,2},{4,5},{5,4},{6,7},{7,6},{8,9},{9,8},{10,11... | collective-permute-start | bytes 393224 | tf_op jit(solution)/shard_map/ppermute | solution.py:34
  97.3 13.3 %collective-permute-start.24 = (bf16[256,640]{1,0:T(8,128)(2,1)S(1)}, bf16[256,640]{1,0:T(8,128)(2,1)S(1)}, u32[]{:S(2)}, u32[]{:S(2)}) collective-permute-start(bf16[256,640]{1,0:T(8,128)(2,1)S(1)} %collective-permute-done.23.refs_19_), channel_id=1, source_target_pairs={{0,16},{16,0},{1,17},{17,1},{2,18},{18,2},{3,19},{19,3},{4,20},{20... | collective-permute-start | bytes 983048 | tf_op jit(solution)/shard_map/ppermute | solution.py:24
  99.1 18.5 %collective-permute-start.26 = (bf16[256,640]{1,0:T(8,128)(2,1)S(1)}, bf16[256,640]{1,0:T(8,128)(2,1)S(1)}, u32[]{:S(2)}, u32[]{:S(2)}) collective-permute-start(bf16[256,640]{1,0:T(8,128)(2,1)S(1)} %collective-permute-done.25.refs_21_), channel_id=1, source_target_pairs={{0,16},{16,0},{1,17},{17,1},{2,18},{18,2},{3,19},{19,3},{4,20},{20... | collective-permute-start | bytes 983048 | tf_op jit(solution)/shard_map/ppermute | solution.py:24
  100.6 1.3 collective-permute-start.16
  100.6 1.5 collective-permute-start.17
  102.0 17.2 %collective-permute-start.18 = (bf16[32,2048]{1,0:T(8,128)(2,1)S(1)}, bf16[32,2048]{1,0:T(8,128)(2,1)S(1)}, u32[]{:S(2)}, u32[]{:S(2)}) collective-permute-start(bf16[32,2048]{1,0:T(8,128)(2,1)S(1)} %collective-permute-done.10.refs_5_), channel_id=1, source_target_pairs={{0,1},{1,0},{2,3},{3,2},{4,5},{5,4},{6,7},{7,6},{8,9},{9,8},{10,11... | collective-permute-start | bytes 393224 | tf_op jit(solution)/shard_map/ppermute | solution.py:34
  102.1 17.5 %collective-permute-start.19 = (bf16[32,2048]{1,0:T(8,128)(2,1)S(1)}, bf16[32,2048]{1,0:T(8,128)(2,1)S(1)}, u32[]{:S(2)}, u32[]{:S(2)}) collective-permute-start(bf16[32,2048]{1,0:T(8,128)(2,1)S(1)} %collective-permute-done.11.refs_6_), channel_id=1, source_target_pairs={{0,1},{1,0},{2,3},{3,2},{4,5},{5,4},{6,7},{7,6},{8,9},{9,8},{10,11... | collective-permute-start | bytes 393224 | tf_op jit(solution)/shard_map/ppermute | solution.py:34
  103.6 16.1 %collective-permute-start.20 = (bf16[32,2048]{1,0:T(8,128)(2,1)S(1)}, bf16[32,2048]{1,0:T(8,128)(2,1)S(1)}, u32[]{:S(2)}, u32[]{:S(2)}) collective-permute-start(bf16[32,2048]{1,0:T(8,128)(2,1)S(1)} %collective-permute-done.12.refs_7_), channel_id=1, source_target_pairs={{0,1},{1,0},{2,3},{3,2},{4,5},{5,4},{6,7},{7,6},{8,9},{9,8},{10,11... | collective-permute-start | bytes 393224 | tf_op jit(solution)/shard_map/ppermute | solution.py:34
  110.6 12.2 %collective-permute-start.28 = (bf16[128,640]{1,0:T(8,128)(2,1)S(1)}, bf16[128,640]{1,0:T(8,128)(2,1)S(1)}, u32[]{:S(2)}, u32[]{:S(2)}) collective-permute-start(bf16[128,640]{1,0:T(8,128)(2,1)S(1)} %collective-permute-done.27.refs_2_), channel_id=1, source_target_pairs={{0,16},{16,0},{1,17},{17,1},{2,18},{18,2},{3,19},{19,3},{4,20},{20... | collective-permute-start | bytes 491528 | tf_op jit(solution)/shard_map/ppermute | solution.py:24
  117.6 7.1 %collective-permute-start.30 = (bf16[128,640]{1,0:T(8,128)(2,1)S(1)}, bf16[128,640]{1,0:T(8,128)(2,1)S(1)}, u32[]{:S(2)}, u32[]{:S(2)}) collective-permute-start(bf16[128,640]{1,0:T(8,128)(2,1)S(1)} %collective-permute-done.29.refs_4_), channel_id=1, source_target_pairs={{0,16},{16,0},{1,17},{17,1},{2,18},{18,2},{3,19},{19,3},{4,20},{20... | collective-permute-start | bytes 491528 | tf_op jit(solution)/shard_map/ppermute | solution.py:24
  119.1 7.4 %collective-permute-start.32 = (bf16[128,640]{1,0:T(8,128)(2,1)S(1)}, bf16[128,640]{1,0:T(8,128)(2,1)S(1)}, u32[]{:S(2)}, u32[]{:S(2)}) collective-permute-start(bf16[128,640]{1,0:T(8,128)(2,1)S(1)} %collective-permute-done.31.refs_6_), channel_id=1, source_target_pairs={{0,16},{16,0},{1,17},{17,1},{2,18},{18,2},{3,19},{19,3},{4,20},{20... | collective-permute-start | bytes 491528 | tf_op jit(solution)/shard_map/ppermute | solution.py:24
  128.5 2.7 %collective-permute-start.33 = (bf16[256,2048]{1,0:T(8,128)(2,1)S(1)}, bf16[256,2048]{1,0:T(8,128)(2,1)S(1)}, u32[]{:S(2)}, u32[]{:S(2)}) collective-permute-start(bf16[256,2048]{1,0:T(8,128)(2,1)S(1)} %get-tuple-element.34), channel_id=1, source_target_pairs={{0,1},{1,0},{2,3},{3,2},{4,5},{5,4},{6,7},{7,6},{8,9},{9,8},{10,11... | collective-permute-start | bytes 3145736 | tf_op jit(solution)/shard_map/ppermute | solution.py:34
  131.6 6.4 %collective-permute-start.34 = (bf16[1,32,2048]{2,1,0:T(8,128)(2,1)S(1)}, bf16[1,32,2048]{2,1,0:T(8,128)(2,1)S(1)}, u32[]{:S(2)}, u32[]{:S(2)}) collective-permute-start(bf16[1,32,2048]{2,1,0:T(8,128)(2,1)S(1)} %fusion.24), channel_id=1, source_target_pairs={{0,2},{1,3},{2,0},{3,1},{4,6},{5,7},{6,4},{7,5},{8,10},{9,11},{10,... | collective-permute-start | bytes 393224 | tf_op jit(solution)/shard_map/ppermute | solution.py:34
  133.2 7.7 %collective-permute-start.36 = (bf16[1,32,2048]{2,1,0:T(8,128)(2,1)S(1)}, bf16[1,32,2048]{2,1,0:T(8,128)(2,1)S(1)}, u32[]{:S(2)}, u32[]{:S(2)}) collective-permute-start(bf16[1,32,2048]{2,1,0:T(8,128)(2,1)S(1)} %fusion.26), channel_id=1, source_target_pairs={{0,2},{1,3},{2,0},{3,1},{4,6},{5,7},{6,4},{7,5},{8,10},{9,11},{10,... | collective-permute-start | bytes 393224 | tf_op jit(solution)/shard_map/ppermute | solution.py:34
  133.8 9.9 %collective-permute-start.38 = (bf16[1,32,2048]{2,1,0:T(8,128)(2,1)S(1)}, bf16[1,32,2048]{2,1,0:T(8,128)(2,1)S(1)}, u32[]{:S(2)}, u32[]{:S(2)}) collective-permute-start(bf16[1,32,2048]{2,1,0:T(8,128)(2,1)S(1)} %fusion.28), channel_id=1, source_target_pairs={{0,2},{1,3},{2,0},{3,1},{4,6},{5,7},{6,4},{7,5},{8,10},{9,11},{10,... | collective-permute-start | bytes 393224 | tf_op jit(solution)/shard_map/ppermute | solution.py:34
  135.4 17.9 %copy-start.13 = (f32[2048]{0:T(1024)S(1)}, f32[2048]{0:T(1024)}, u32[]{:S(2)}) copy-start(f32[2048]{0:T(1024)} %param.20) | copy-start | bytes 24580
  135.4 11.5 %collective-permute-start.40 = (bf16[1,32,2048]{2,1,0:T(8,128)(2,1)S(1)}, bf16[1,32,2048]{2,1,0:T(8,128)(2,1)S(1)}, u32[]{:S(2)}, u32[]{:S(2)}) collective-permute-start(bf16[1,32,2048]{2,1,0:T(8,128)(2,1)S(1)} %fusion.29), channel_id=1, source_target_pairs={{0,2},{1,3},{2,0},{3,1},{4,6},{5,7},{6,4},{7,5},{8,10},{9,11},{10,... | collective-permute-start | bytes 393224 | tf_op jit(solution)/shard_map/ppermute | solution.py:34
  138.1 8.8 %collective-permute-start.35 = (bf16[32,2048]{1,0:T(8,128)(2,1)S(1)}, bf16[32,2048]{1,0:T(8,128)(2,1)S(1)}, u32[]{:S(2)}, u32[]{:S(2)}) collective-permute-start(bf16[32,2048]{1,0:T(8,128)(2,1)S(1)} %fusion.23), channel_id=1, source_target_pairs={{0,12},{4,0},{8,4},{12,8},{1,13},{5,1},{9,5},{13,9},{2,14},{6,2},{... | collective-permute-start | bytes 393224 | tf_op jit(solution)/shard_map/ppermute | solution.py:24
  140.9 12.1 %collective-permute-start.37 = (bf16[32,2048]{1,0:T(8,128)(2,1)S(1)}, bf16[32,2048]{1,0:T(8,128)(2,1)S(1)}, u32[]{:S(2)}, u32[]{:S(2)}) collective-permute-start(bf16[32,2048]{1,0:T(8,128)(2,1)S(1)} %fusion.25), channel_id=1, source_target_pairs={{0,8},{4,12},{8,0},{12,4},{1,9},{5,13},{9,1},{13,5},{2,10},{6,14},... | collective-permute-start | bytes 393224 | tf_op jit(solution)/shard_map/ppermute | solution.py:24
  143.7 9.3 %collective-permute-start.39 = (bf16[32,2048]{1,0:T(8,128)(2,1)S(1)}, bf16[32,2048]{1,0:T(8,128)(2,1)S(1)}, u32[]{:S(2)}, u32[]{:S(2)}) collective-permute-start(bf16[32,2048]{1,0:T(8,128)(2,1)S(1)} %fusion.27), channel_id=1, source_target_pairs={{0,4},{4,8},{8,12},{12,0},{1,5},{5,9},{9,13},{13,1},{2,6},{6,10},{... | collective-permute-start | bytes 393224 | tf_op jit(solution)/shard_map/ppermute | solution.py:24
  153.3 5.0 %collective-permute-start.42 = (bf16[32,2048]{1,0:T(8,128)(2,1)S(1)}, bf16[32,2048]{1,0:T(8,128)(2,1)S(1)}, u32[]{:S(2)}, u32[]{:S(2)}) collective-permute-start(bf16[32,2048]{1,0:T(8,128)(2,1)S(1)} %fusion.9.refs_0_), channel_id=1, source_target_pairs={{0,2},{1,3},{2,0},{3,1},{4,6},{5,7},{6,4},{7,5},{8,10},{9,11},{10,... | collective-permute-start | bytes 393224 | tf_op jit(solution)/shard_map/ppermute | solution.py:34
  154.6 3.8 %collective-permute-start.41 = (bf16[32,2048]{1,0:T(8,128)(2,1)S(1)}, bf16[32,2048]{1,0:T(8,128)(2,1)S(1)}, u32[]{:S(2)}, u32[]{:S(2)}) collective-permute-start(bf16[32,2048]{1,0:T(8,128)(2,1)S(1)} %fusion.9.refs_0_), channel_id=1, source_target_pairs={{0,1},{1,0},{2,3},{3,2},{4,5},{5,4},{6,7},{7,6},{8,9},{9,8},{10,11... | collective-permute-start | bytes 393224 | tf_op jit(solution)/shard_map/ppermute | solution.py:34
  158.4 1.3 collective-permute-start.43
  (10 other events, 43.2 us)
where the time goes:
time: 163 us; the launch traced here: 162 us
  waiting for transfers between devices  82.9 us (51%)
  starting transfers between devices  52.8 us (32%)
  Pallas kernels  18.1 us (11%)
  other arithmetic  3.6 us (2%)
  local copies, waits for them, and re-layouts  3.45 us (2%)
    ppermute x18, waiting for transfers between devices, shift(): lax.ppermute(rows, axis, [(i, (i + step) % count) for i in range(count)])  63 us
    ppermute x18, starting transfers between devices, shift(): lax.ppermute(rows, axis, [(i, (i + step) % count) for i in range(count)])  28.1 us
    pallas_call x7, Pallas kernels, call(): pl.pallas_call(kernel, out_shape=outs, in_specs=specs, out_specs=out_spec...  18.1 us
    ppermute x23, waiting for transfers between devices, swap(): return lax.ppermute(rows, axis, [(i, i ^ bit) for i in range(count)])  14.9 us
    ppermute x23, starting transfers between devices, swap(): return lax.ppermute(rows, axis, [(i, i ^ bit) for i in range(count)])  14 us
    ppermute x3, starting transfers between devices, upward(): lax.ppermute(rows, axis, [(i, i + step) for i in range(count - step)])  10.7 us
    ppermute x3, waiting for transfers between devices, upward(): lax.ppermute(rows, axis, [(i, i + step) for i in range(count - step)])  4.97 us
  transfers between devices with their start and end apart: 44, of which 22 were waited for; matrix products, arithmetic and copies ran while one was open for 2% of the time, Pallas kernels for 5%

commit v1 on v0

--- a/solution.py
+++ b/solution.py
@@ -34,9 +34,8 @@
     return lax.ppermute(rows, axis, [(i, i ^ bit) for i in range(count)])
 
 
-def call(kernel, outs, flops, *args, scalars=0, scratch=(), limit=None):
-    specs = [pl.BlockSpec(memory_space=pltpu.SMEM)] * scalars
-    specs += [pl.BlockSpec(memory_space=pltpu.VMEM)] * (len(args) - scalars)
+def call(kernel, outs, flops, *args, scratch=(), limit=None):
+    specs = [pl.BlockSpec(memory_space=pltpu.VMEM)] * len(args)
     single = not isinstance(outs, list)
     out_list = [outs] if single else outs
     moved = sum(a.size * a.dtype.itemsize for a in (*args, *out_list))
@@ -60,7 +59,11 @@
     tok_rows, width = key_ref.shape
     out_ref[:tok_rows, :width] = key_ref[...]
     out_ref[:tok_rows, width:] = value_ref[...]
-    out_ref[tok_rows:, :tok_rows] = logit_ref[...]
+    head_count = logit_ref.shape[1]
+    row = lax.broadcasted_iota(jnp.int32, (pad_rows, head_count), 0)
+    column = lax.broadcasted_iota(jnp.int32, (pad_rows, head_count), 1)
+    pick = (row == column).astype(jnp.float32).astype(jnp.bfloat16)
+    out_ref[tok_rows:, :tok_rows] = dot_t(pick, logit_ref[...]).astype(out_ref.dtype)
     out_ref[tok_rows:, tok_rows:] = jnp.zeros((pad_rows, 2 * width - tok_rows), out_ref.dtype)
 
 
@@ -111,14 +114,13 @@
     tok_rows, width = queries.shape
     head_count = logit_part.shape[1]
     ring = lax.axis_size("sp")
-    logit_rows = jnp.pad(jnp.transpose(logit_part), ((0, pad_rows - head_count), (0, 0)))
     packed = call(
         pack_kernel,
         jax.ShapeDtypeStruct((tok_rows + pad_rows, 2 * width), key_part.dtype),
         1,
         key_part,
         value_part,
-        logit_rows,
+        logit_part,
     )
     blocks = [packed] + [upward(packed, "sp", step) for step in range(1, ring)]
     attended = call(
@@ -169,69 +171,82 @@
     return jnp.where(lower, low, high).astype(jnp.bfloat16)
 
 
-def pack_wide_kernel(ring, where_ref, gate_ref, up_ref, own_ref, *out_refs):
-    own, copy = where_ref[0], where_ref[1]
-    share = out_refs[0].shape[0]
-    for step in range(ring):
+def pack_wide(out, gate_ref, up_ref, rows, ring, target):
+    gate, up = main_at(gate_ref, rows, ring, target), main_at(up_ref, rows, ring, target)
+    count, main = gate.shape
+    out[:count, :main] = gate
+    out[:count, main : 2 * main] = up
+    out[:count, 2 * main :] = halves(
+        tile_at(gate_ref, rows, ring, target),
+        tile_at(up_ref, rows, ring, target),
+        target % 2 == 1,
+    )
+
+
+def pack_narrow(out, place, down_ref, start, half, ring, target):
+    upper = pl.ds(pl.multiple_of(start, half), half)
+    lower = pl.ds(pl.multiple_of(start + half, half), half)
+    main = (out.shape[1] - lanes) // 2
+    rows = slice(place, place + half)
+    out[rows, :main] = main_at(down_ref, upper, ring, target)
+    out[rows, main : 2 * main] = main_at(down_ref, lower, ring, target)
+    out[rows, 2 * main :] = halves(
+        tile_at(down_ref, upper, ring, target),
+        tile_at(down_ref, lower, ring, target),
+        target % 2 == 1,
+    )
+
+
+def pack_outer_kernel(ring, steps, gate_ref, up_ref, down_ref, *out_refs):
+    own, copy = lax.axis_index("sp"), lax.axis_index("grp")
+    for step, out in zip(steps, out_refs):
+        share = out.shape[0] // 3 * 2
         target = lax.rem(own + step, ring)
-        out = own_ref if step == 0 else out_refs[step - 1]
-        rows = slice(None) if step == 0 else pl.ds(pl.multiple_of(copy * share, share), share)
-        gate, up = main_at(gate_ref, rows, ring, target), main_at(up_ref, rows, ring, target)
-        main = gate.shape[1]
-        out[:, :main] = gate
-        out[:, main : 2 * main] = up
-        out[:, 2 * main :] = halves(
-            tile_at(gate_ref, rows, ring, target),
-            tile_at(up_ref, rows, ring, target),
-            target % 2 == 1,
-        )
-
-
-def pack_narrow_kernel(ring, where_ref, down_ref, *out_refs):
-    own, copy = where_ref[0], where_ref[1]
-    half = out_refs[0].shape[0]
-    copies = down_ref.shape[0] // (2 * half)
-    for step in range(1 - copies, ring):
-        target = lax.rem(own + max(step, 0), ring)
-        out = out_refs[step + copies - 1]
-        start = (step + copies - 1) * 2 * half if step <= 0 else copy * 2 * half
-        upper = pl.ds(pl.multiple_of(start, half), half)
-        lower = pl.ds(pl.multiple_of(start + half, half), half)
-        main = (out.shape[1] - lanes) // 2
-        out[:, :main] = main_at(down_ref, upper, ring, target)
-        out[:, main : 2 * main] = main_at(down_ref, lower, ring, target)
-        out[:, 2 * main :] = halves(
-            tile_at(down_ref, upper, ring, target),
-            tile_at(down_ref, lower, ring, target),
-            target % 2 == 1,
-        )
-
-
-def exchange(pieces):
-    copies = lax.axis_size("grp")
-    arrived = []
-    for step, piece in enumerate(pieces, 1):
-        piece = shift(piece, "sp", step)
-        arrived.append([piece] + [shift(piece, "grp", turn) for turn in range(1, copies)])
-    return arrived
-
-
-def wide_kernel(ring, copies, block_count, where_ref, *refs):
+        start = pl.multiple_of(copy * share, share)
+        pack_wide(out, gate_ref, up_ref, pl.ds(start, share), ring, target)
+        pack_narrow(out, share, down_ref, start, share // 2, ring, target)
+
+
+def pack_middle_kernel(ring, step, gate_ref, up_ref, down_ref, wide_ref, narrow_ref):
+    own, copy = lax.axis_index("sp"), lax.axis_index("grp")
+    share = wide_ref.shape[0]
+    target = lax.rem(own + step, ring)
+    start = pl.multiple_of(copy * share, share)
+    pack_wide(wide_ref, gate_ref, up_ref, pl.ds(start, share), ring, target)
+    pack_narrow(narrow_ref, 0, down_ref, start, share // 2, ring, target)
+
+
+def pack_own_kernel(ring, gate_ref, up_ref, down_ref, wide_ref, narrow_ref):
+    own = lax.axis_index("sp")
+    share = wide_ref.shape[0] // lax.axis_size("grp")
+    pack_wide(wide_ref, gate_ref, up_ref, slice(None), ring, own)
+    for copy in range(lax.axis_size("grp")):
+        place = copy * share // 2
+        pack_narrow(narrow_ref, place, down_ref, copy * share, share // 2, ring, own)
+
+
+def exchange(piece, step):
+    piece = shift(piece, "sp", step)
+    turns = range(1, lax.axis_size("grp"))
+    return [piece] + [shift(piece, "grp", turn) for turn in turns]
+
+
+def wide_kernel(ring, copies, block_count, *refs):
     blocks, refs = refs[:block_count], refs[block_count:]
     own_ref, pieces, (low_ref, high_ref), scratch = refs[0], refs[1:-4], refs[-4:-2], refs[-2:]
     weight, rows_ref = scratch
-    own, copy = where_ref[0], where_ref[1]
+    own, copy = lax.axis_index("sp"), lax.axis_index("grp")
     block_rows = blocks[0].shape[0]
     for index, block in enumerate(blocks):
         rows_ref[index * block_rows : (index + 1) * block_rows, :] = block[...]
-    depth, share = own_ref.shape[0], pieces[0].shape[0]
+    depth, share = own_ref.shape[0], own_ref.shape[0] // copies
     weight[pl.ds(pl.multiple_of(own * depth, depth), depth), :] = own_ref[...]
     for step in range(1, ring):
         for turn in range(copies):
             source = lax.rem(own - step + ring, ring)
             place = lax.rem(copy - turn + copies, copies)
             start = pl.multiple_of(source * depth + place * share, share)
-            weight[pl.ds(start, share), :] = pieces[(step - 1) * copies + turn][...]
+            weight[pl.ds(start, share), :] = pieces[(step - 1) * copies + turn][:share]
     main = (own_ref.shape[1] - lanes) // 2
     count = rows_ref.shape[0]
     tile = min(count, 256)
@@ -255,41 +270,40 @@
     lax.fori_loop(0, count // tile, body, 0)
 
 
-def narrow_kernel(ring, copies, where_ref, low_ref, high_ref, *refs):
-    own_refs, pieces, outs, weights = refs[:copies], refs[copies:-4], refs[-4:-2], refs[-2:]
-    own, copy = where_ref[0], where_ref[1]
-    half = own_refs[0].shape[0]
-    main = (own_refs[0].shape[1] - lanes) // 2
-
-    def place_piece(ref, source, place):
+def narrow_kernel(ring, copies, low_ref, high_ref, own_ref, *refs):
+    pieces, weights = refs[: copies * (ring - 1)], refs[-2:]
+    outs = refs[copies * (ring - 1) : -2]
+    own, copy = lax.axis_index("sp"), lax.axis_index("grp")
+    half = own_ref.shape[0] // copies
+    main = (own_ref.shape[1] - lanes) // 2
+
+    def place_piece(ref, first, source, place):
         start = pl.multiple_of((source * copies + place) * half, half)
+        rows = slice(first, first + half)
         for part, weight in enumerate(weights):
-            weight[pl.ds(start, half), :main] = ref[:, part * main : (part + 1) * main]
-            weight[pl.ds(start, half), main:] = ref[:, 2 * main :]
+            weight[pl.ds(start, half), :main] = ref[rows, part * main : (part + 1) * main]
+            weight[pl.ds(start, half), main:] = ref[rows, 2 * main :]
 
     for place in range(copies):
-        place_piece(own_refs[place], own, place)
+        place_piece(own_ref, place * half, own, place)
     for step in range(1, ring):
         for turn in range(copies):
             source = lax.rem(own - step + ring, ring)
             place = lax.rem(copy - turn + copies, copies)
-            place_piece(pieces[(step - 1) * copies + turn], source, place)
+            piece = pieces[(step - 1) * copies + turn]
+            place_piece(piece, piece.shape[0] - half, source, place)
     count = outs[0].shape[0]
-    for index, out in enumerate(outs):
-        rows = slice(index * count, (index + 1) * count)
+    for index in range(2):
+        rows = slice(index * count * ring, (index + 1) * count * ring)
         for part, hidden_ref in enumerate((low_ref, high_ref)):
             units = dot_t(hidden_ref[rows, :], weights[part][...]).astype(jnp.bfloat16)
-            for block in range(ring * copies):
-                start = (2 * block + part) * half
-                out[:, start : start + half] = units[:, block * half : (block + 1) * half]
-
-
-def join_kernel(member_ref, *refs):
-    parts, out_ref = refs[:-1], refs[-1]
-    rows = parts[0].shape[0]
-    for offset, part in enumerate(parts):
-        start = pl.multiple_of((member_ref[0] ^ offset) * rows, rows)
-        out_ref[pl.ds(start, rows), :] = part[...]
+            for step in range(ring):
+                out = outs[index * ring + step]
+                for block in range(ring * copies):
+                    start = (2 * block + part) * half
+                    out[:, start : start + half] = units[
+                        step * count : (step + 1) * count, block * half : (block + 1) * half
+                    ]
 
 
 def shards(
@@ -306,8 +320,8 @@
     up_weight,
     down_weight,
 ):
-    ring, own = lax.axis_size("sp"), lax.axis_index("sp")
-    copies, copy = lax.axis_size("grp"), lax.axis_index("grp")
+    ring = lax.axis_size("sp")
+    copies = lax.axis_size("grp")
     members, member = lax.axis_size("tp"), lax.axis_index("tp")
     tok_rows, width = residual.shape
     own_rows = tok_rows // members
@@ -315,23 +329,43 @@
     depth, part = gate_weight.shape[0], gate_weight.shape[1] // ring
     main, share = part // lanes * lanes, depth // copies
     packs = main > 0 and 2 * (part - main) == lanes and ring % 2 == 0 and share % 32 == 0
-    where = jnp.stack([own, copy]).astype(jnp.int32)
 
     attended, packed = attend(query_rows, key_rows, value_rows, key_logit)
     if packs:
-        shape = jax.ShapeDtypeStruct
+        wide, narrow = [None] * ring, [None] * ring
+        outer = [step for step in range(1, ring) if step != ring // 2]
+
+        def pack(kernel, rows, *weights):
+            shapes = [jax.ShapeDtypeStruct((count, 2 * part), jnp.bfloat16) for count in rows]
+            return call(kernel, shapes, 1, *weights)
+
         gate_in, up_in, _ = lax.optimization_barrier((gate_weight, up_weight, packed))
-        wide_own, *wide = call(
-            functools.partial(pack_wide_kernel, ring),
-            [shape((depth, 2 * part), jnp.bfloat16)]
-            + [shape((share, 2 * part), jnp.bfloat16)] * (ring - 1),
-            1,
-            where,
+        pieces = pack(
+            functools.partial(pack_outer_kernel, ring, outer),
+            [share // 2 * 3] * len(outer),
             gate_in,
             up_in,
-            scalars=1,
+            down_weight,
         )
-        wide = [piece for group in exchange(wide) for piece in group]
+        for step, piece in zip(outer, pieces):
+            wide[step] = narrow[step] = exchange(piece, step)
+        middle_wide, middle_narrow = pack(
+            functools.partial(pack_middle_kernel, ring, ring // 2),
+            [share, share // 2],
+            gate_weight,
+            up_weight,
+            down_weight,
+        )
+        wide[ring // 2] = exchange(middle_wide, ring // 2)
+        narrow[ring // 2] = exchange(middle_narrow, ring // 2)
+        wide_own, narrow_own = pack(
+            functools.partial(pack_own_kernel, ring),
+            [depth, depth // 2],
+            gate_weight,
+            up_weight,
+            down_weight,
+        )
+        wide, narrow = sum(wide[1:], []), sum(narrow[1:], [])
 
     head_part = jnp.dot(attended, out_weight, preferred_element_type=jnp.float32)
     head_part = head_part.astype(jnp.bfloat16).reshape(members, own_rows, width)
@@ -348,58 +382,44 @@
     normed = (ffn_gain * normalize(middle.astype(jnp.float32))).astype(jnp.bfloat16)
 
     if packs:
-        narrow = call(
-            functools.partial(pack_narrow_kernel, ring),
-            [shape((share // 2, 2 * part), jnp.bfloat16)] * (ring - 1 + copies),
-            1,
-            where,
-            down_weight,
-            scalars=1,
-        )
-        narrow_own, narrow = narrow[:copies], narrow[copies:]
-        narrow = [piece for group in exchange(narrow) for piece in group]
-
+        shape = jax.ShapeDtypeStruct
         blocks = {(0, 0): normed}
         for step in range(1, ring):
             blocks[0, step] = shift(normed, "sp", step)
         for bit in reversed(bits):
             for (offset, step), block in list(blocks.items()):
                 blocks[offset ^ bit, step] = swap(block, "tp", bit)
-        order = [(2 * p + half, k) for half in range(2) for p in range(members // 2) for k in range(ring)]
+        order = [(2 * p + half, k) for half in range(2) for k in range(ring) for p in range(members // 2)]
         all_rows = len(order) * own_rows
         hidden = call(
             functools.partial(wide_kernel, ring, copies, len(order)),
             [shape((all_rows, main + lanes), jnp.bfloat16)] * 2,
             4 * all_rows * width * part,
-            where,
             *[blocks[key] for key in order],
             wide_own,
             *wide,
-            scalars=1,
             scratch=[
                 pltpu.VMEM((width, 2 * part), jnp.bfloat16),
                 pltpu.VMEM((all_rows, width), jnp.bfloat16),
             ],
             limit=40 << 20,
         )
-        kept, sent = call(
+        units_out = call(
             functools.partial(narrow_kernel, ring, copies),
-            [shape((all_rows // 2, width), jnp.bfloat16)] * 2,
+            [shape((all_rows // (2 * ring), width), jnp.bfloat16)] * (2 * ring),
             2 * all_rows * width * part,
-            where,
             *hidden,
-            *narrow_own,
+            narrow_own,
             *narrow,
-            scalars=1,
             scratch=[pltpu.VMEM((width // 2, main + lanes), jnp.bfloat16)] * 2,
             limit=40 << 20,
         )
-        arrived = swap(sent, "tp", 1)
-        kept = kept.reshape(members // 2, ring, own_rows, width)
-        arrived = arrived.reshape(members // 2, ring, own_rows, width)
         ffn_out = jnp.zeros((own_rows, width), jnp.float32)
-        for step in [*range(1, ring), 0]:
-            units = kept[:, step].astype(jnp.float32) + arrived[:, step].astype(jnp.float32)
+        for step in sorted(range(ring), key=lambda k: (k == 0, abs(2 * k - ring))):
+            kept, sent = units_out[step], units_out[ring + step]
+            sent = swap(sent, "tp", 1)
+            units = kept.astype(jnp.float32) + sent.astype(jnp.float32)
+            units = units.reshape(members // 2, own_rows, width)
             for bit in bits[1:]:
                 moved = swap(units[1::2].astype(jnp.bfloat16), "tp", bit)
                 units = units[0::2] + moved.astype(jnp.float32)
@@ -438,14 +458,10 @@
     for bit in reversed(bits):
         for offset, rows in list(parts.items()):
             parts[offset ^ bit] = swap(rows, "tp", bit)
-    return call(
-        join_kernel,
-        jax.ShapeDtypeStruct((tok_rows, width), jnp.bfloat16),
-        1,
-        member[None].astype(jnp.int32),
-        *[parts[offset] for offset in range(members)],
-        scalars=1,
-    )
+    result = jnp.zeros((tok_rows, width), jnp.bfloat16)
+    for offset in range(members):
+        result = lax.dynamic_update_slice(result, parts[offset], ((member ^ offset) * own_rows, 0))
+    return result
 
 
 def solution(mesh):

time: 163 us -> 181 us (1.11)
  local copies, waits for them, and re-layouts: 3.45 us -> 22.9 us
  starting transfers between devices: 52.8 us -> 43.3 us
  waiting for transfers between devices: 82.9 us -> 89.5 us
  Pallas kernels: 18.1 us -> 21.4 us
    unnamed x28 -> x73, local copies, waits for them, and re-layouts: 1.35 us -> 22.1 us
    ppermute x18 -> x14, starting transfers between devices: 28.1 us -> 18.5 us  [shift(): lax.ppermute(rows, axis, [(i, (i + step) % count) for i in range(count)])]
    ppermute x18 -> x14, waiting for transfers between devices: 63 us -> 70 us  [shift(): lax.ppermute(rows, axis, [(i, (i + step) % count) for i in range(count)])]
    pallas_call x7, Pallas kernels: 18.1 us -> 21.4 us  [call(): pl.pallas_call(kernel, out_shape=outs, in_specs=specs, out_specs=out_spec...]
    ppermute x23 -> x26, waiting for transfers between devices: 14.9 us -> 14.5 us  [swap(): return lax.ppermute(rows, axis, [(i, i ^ bit) for i in range(count)])]
    ppermute x23 -> x26, starting transfers between devices: 14 us -> 14 us  [swap(): return lax.ppermute(rows, axis, [(i, i ^ bit) for i in range(count)])]
  transfers between devices with their start and end apart: 44 -> 43, of which waited for: 22 -> 19; matrix products, arithmetic and copies ran while one was open for 2% -> 1% of each run, Pallas kernels for 5% -> 7%
where the time goes in v1:
time: 181 us
  waiting for transfers between devices  89.5 us (49%)
  starting transfers between devices  43.3 us (24%)
  local copies, waits for them, and re-layouts  22.9 us (13%)
  Pallas kernels  21.4 us (12%)
  other arithmetic  2.08 us (1%)
    ppermute x14, waiting for transfers between devices, shift(): lax.ppermute(rows, axis, [(i, (i + step) % count) for i in range(count)])  70 us
    unnamed x73, local copies, waits for them, and re-layouts  22.1 us
    pallas_call x7, Pallas kernels, call(): pl.pallas_call(kernel, out_shape=outs, in_specs=specs, out_specs=out_spec...  21.4 us
    ppermute x14, starting transfers between devices, shift(): lax.ppermute(rows, axis, [(i, (i + step) % count) for i in range(count)])  18.5 us
    ppermute x26, waiting for transfers between devices, swap(): return lax.ppermute(rows, axis, [(i, i ^ bit) for i in range(count)])  14.5 us
    ppermute x26, starting transfers between devices, swap(): return lax.ppermute(rows, axis, [(i, i ^ bit) for i in range(count)])  14 us
    ppermute x3, starting transfers between devices, upward(): lax.ppermute(rows, axis, [(i, i + step) for i in range(count - step)])  10.7 us
    ppermute x3, waiting for transfers between devices, upward(): lax.ppermute(rows, axis, [(i, i + step) for i in range(count - step)])  4.97 us
  transfers between devices with their start and end apart: 43, of which 19 were waited for; matrix products, arithmetic and copies ran while one was open for 1% of the time, Pallas kernels for 7%

profile of v1, /device:TPU:0, one launch (start us, length us, event | category | flops | bytes accessed | tf_op | source)
XLA Modules:
  0.0 180.7 jit_solution(9288067124659646110)
XLA Ops:
  0.0 1.5 copy.13.logit_ref
  1.5 1.7 shard_map.118.refs_0_
  3.1 5.0 %collective-permute-start = (bf16[144,512]{1,0:T(8,128)(2,1)}, bf16[144,512]{1,0:T(8,128)(2,1)S(1)}, u32[]{:S(2)}, u32[]{:S(2)}) collective-permute-start(bf16[144,512]{1,0:T(8,128)(2,1)} %shard_map.118.refs_0_), channel_id=1, source_target_pairs={{0,4},{4,8},{8,12},{1,5},{5,9},{9,13},{2,6},{6,10},{10,14},{3,7},{... | collective-permute-start | bytes 442376 | tf_op jit(solution)/shard_map/ppermute | solution.py:29
  8.1 4.5 %collective-permute-start.1 = (bf16[144,512]{1,0:T(8,128)(2,1)}, bf16[144,512]{1,0:T(8,128)(2,1)S(1)}, u32[]{:S(2)}, u32[]{:S(2)}) collective-permute-start(bf16[144,512]{1,0:T(8,128)(2,1)} %shard_map.118.refs_0_), channel_id=1, source_target_pairs={{0,8},{4,12},{1,9},{5,13},{2,10},{6,14},{3,11},{7,15},{16,24},{20,... | collective-permute-start | bytes 442376 | tf_op jit(solution)/shard_map/ppermute | solution.py:29
  12.6 1.3 collective-permute-start.2
  14.0 3.2 %collective-permute-done.1.refs_2_ = bf16[144,512]{1,0:T(8,128)(2,1)S(1)} collective-permute-done((bf16[144,512]{1,0:T(8,128)(2,1)}, bf16[144,512]{1,0:T(8,128)(2,1)S(1)}, u32[]{:S(2)}, u32[]{:S(2)}) %collective-permute-start.1) | collective-permute-done | bytes 147488 | tf_op jit(solution)/shard_map/ppermute | solution.py:29
  17.1 1.8 collective-permute-done.2.refs_3_
  19.6 4.1 %shard_map.119 = bf16[128,256]{1,0:T(8,128)(2,1)} custom-call(bf16[128,256]{1,0:T(8,128)(2,1)} %query_ref.1, bf16[144,512]{1,0:T(8,128)(2,1)} %shard_map.118.refs_0_, bf16[144,512]{1,0:T(8,128)(2,1)} %copy-done.30, bf16[144,512]{1,0:T(8,128)(2,1)} %copy-done.31, bf16[144,512]{1,0:T(8,128)(2,1)} %copy-done.32), custom_call_target="tpu_custom_call" | custom-call | flops 167772160 | bytes 720896 | tf_op jit(solution)/shard_map/pallas_call | solution.py:43
  23.7 1.1 convolution_convert_fusion
  25.0 1.6 collective-permute-start.4
  26.8 3.2 %shard_map.121 = (bf16[384,640]{1,0:T(8,128)(2,1)}, bf16[384,640]{1,0:T(8,128)(2,1)}) custom-call(bf16[512,1280]{1,0:T(8,128)(2,1)} %gate_ref.4, bf16[512,1280]{1,0:T(8,128)(2,1)} %up_ref.4, bf16[512,1280]{1,0:T(8,128)(2,1)} %down_ref.5), custom_call_target="tpu_custom_call" | custom-call | flops 1 | bytes 4915200 | tf_op jit(solution)/shard_map/pallas_call | solution.py:43
  30.1 4.3 %collective-permute-start.21 = (bf16[384,640]{1,0:T(8,128)(2,1)}, bf16[384,640]{1,0:T(8,128)(2,1)S(1)}, u32[]{:S(2)}, u32[]{:S(2)}) collective-permute-start(bf16[384,640]{1,0:T(8,128)(2,1)} %get-tuple-element.26), channel_id=1, source_target_pairs={{0,4},{4,8},{8,12},{12,0},{1,5},{5,9},{9,13},{13,1},{2,6},{6,10},{... | collective-permute-start | bytes 1474568 | tf_op jit(solution)/shard_map/ppermute | solution.py:24
  34.3 2.8 %collective-permute-start.25 = (bf16[384,640]{1,0:T(8,128)(2,1)}, bf16[384,640]{1,0:T(8,128)(2,1)S(1)}, u32[]{:S(2)}, u32[]{:S(2)}) collective-permute-start(bf16[384,640]{1,0:T(8,128)(2,1)} %get-tuple-element.28), channel_id=1, source_target_pairs={{0,12},{4,0},{8,4},{12,8},{1,13},{5,1},{9,5},{13,9},{2,14},{6,2},{... | collective-permute-start | bytes 1474568 | tf_op jit(solution)/shard_map/ppermute | solution.py:24
  37.1 3.0 %shard_map.122 = (bf16[256,640]{1,0:T(8,128)(2,1)}, bf16[128,640]{1,0:T(8,128)(2,1)}) custom-call(bf16[512,1280]{1,0:T(8,128)(2,1)} %gate_ref.4, bf16[512,1280]{1,0:T(8,128)(2,1)} %up_ref.4, bf16[512,1280]{1,0:T(8,128)(2,1)} %down_ref.5), custom_call_target="tpu_custom_call" | custom-call | flops 1 | bytes 4423680 | tf_op jit(solution)/shard_map/pallas_call | solution.py:43
  40.7 2.4 %collective-permute-start.27 = (bf16[128,640]{1,0:T(8,128)(2,1)}, bf16[128,640]{1,0:T(8,128)(2,1)}, u32[]{:S(2)}, u32[]{:S(2)}) collective-permute-start(bf16[128,640]{1,0:T(8,128)(2,1)} %get-tuple-element.32), channel_id=1, source_target_pairs={{0,8},{4,12},{8,0},{12,4},{1,9},{5,13},{9,1},{13,5},{2,10},{6,14},... | collective-permute-start | bytes 491528 | tf_op jit(solution)/shard_map/ppermute | solution.py:24
  43.3 1.1 fusion.6
  44.6 41.7 %collective-permute-done.27.refs_2_ = bf16[128,640]{1,0:T(8,128)(2,1)} collective-permute-done((bf16[128,640]{1,0:T(8,128)(2,1)}, bf16[128,640]{1,0:T(8,128)(2,1)}, u32[]{:S(2)}, u32[]{:S(2)}) %collective-permute-start.27) | collective-permute-done | bytes 163872 | tf_op jit(solution)/shard_map/ppermute | solution.py:24
  86.3 1.6 collective-permute-start.6
  87.9 5.7 %collective-permute-done.9.refs_4_ = bf16[32,2048]{1,0:T(8,128)(2,1)S(1)} collective-permute-done((bf16[32,2048]{1,0:T(8,128)(2,1)S(1)}, bf16[32,2048]{1,0:T(8,128)(2,1)S(1)}, u32[]{:S(2)}, u32[]{:S(2)}) %collective-permute-start.9) | collective-permute-done | bytes 131104 | tf_op jit(solution)/shard_map/ppermute | solution.py:24
  93.6 1.0 collective-permute-done.11.refs_6_
  94.6 1.5 collective-permute-start.8
  97.3 1.5 collective-permute-start.12
  98.8 1.5 collective-permute-start.22
  101.0 1.5 collective-permute-start.24
  102.5 1.4 collective-permute-done.10.refs_5_
  111.5 16.7 %collective-permute-done.24.refs_20_ = bf16[256,640]{1,0:T(8,128)(2,1)S(1)} collective-permute-done((bf16[256,640]{1,0:T(8,128)(2,1)S(1)}, bf16[256,640]{1,0:T(8,128)(2,1)S(1)}, u32[]{:S(2)}, u32[]{:S(2)}) %collective-permute-start.24) | collective-permute-done | bytes 327712 | tf_op jit(solution)/shard_map/ppermute | solution.py:24
  129.6 1.5 collective-permute-start.28
  131.1 3.2 %shard_map.120 = (bf16[512,640]{1,0:T(8,128)(2,1)}, bf16[256,640]{1,0:T(8,128)(2,1)}) custom-call(bf16[512,1280]{1,0:T(8,128)(2,1)} %gate_ref.4, bf16[512,1280]{1,0:T(8,128)(2,1)} %up_ref.4, bf16[512,1280]{1,0:T(8,128)(2,1)} %down_ref.5), custom_call_target="tpu_custom_call" | custom-call | flops 1 | bytes 4915200 | tf_op jit(solution)/shard_map/pallas_call | solution.py:43
  134.4 1.1 copy-done.1
  135.5 1.0 copy-done.3
  136.4 0.9 copy-done.6
  137.3 0.9 copy-done.8
  138.2 0.9 copy-done.10
  142.8 0.9 copy-done.20
  143.7 0.9 copy-done.22
  146.4 3.7 %shard_map.123 = (bf16[512,384]{1,0:T(8,128)(2,1)S(1)}, bf16[512,384]{1,0:T(8,128)(2,1)S(1)}) custom-call(bf16[32,2048]{1,0:T(8,128)(2,1)S(1)} %fusion.8.refs_0_, bf16[32,2048]{1,0:T(8,128)(2,1)S(1)} %copy-done.12, bf16[32,2048]{1,0:T(8,128)(2,1)S(1)} %copy-done.6, bf16[32,2048]{1,0:T(8,128)(2,1)S(1)} %copy-done.16, bf16[32,2048]{1,0:T(8,128)(2,1)S(1)} %copy-done.8, ...), custom_call_target="tpu_custom_call" | custom-call | flops 1342177280 | bytes 6160384 | tf_op jit(solution)/shard_map/pallas_call | solution.py:43
  150.1 2.4 %shard_map.124 = (bf16[64,2048]{1,0:T(8,128)(2,1)S(1)}, bf16[64,2048]{1,0:T(8,128)(2,1)S(1)}, bf16[64,2048]{1,0:T(8,128)(2,1)S(1)}, bf16[64,2048]{1,0:T(8,128)(2...) custom-call(bf16[512,384]{1,0:T(8,128)(2,1)S(1)} %get-tuple-element., ...), custom_call_target="tpu_custom_call" | custom-call | flops 671088640 | bytes 5505024 | tf_op jit(solution)/shard_map/pallas_call | solution.py:43
  154.9 1.6 collective-permute-start.33
  157.3 1.6 collective-permute-start.39
  158.8 1.9 %collective-permute-done.30 = bf16[1,32,2048]{2,1,0:T(8,128)(2,1)S(1)} collective-permute-done((bf16[1,32,2048]{2,1,0:T(8,128)(2,1)S(1)}, bf16[1,32,2048]{2,1,0:T(8,128)(2,1)S(1)}, u32[]{:S(2)}, u32[]{:S(2)}) %collective-permute-start.30) | collective-permute-done | bytes 131104 | tf_op jit(solution)/shard_map/ppermute | solution.py:34
  160.9 2.6 %collective-permute-done.33 = bf16[1,32,2048]{2,1,0:T(8,128)(2,1)S(1)} collective-permute-done((bf16[1,32,2048]{2,1,0:T(8,128)(2,1)S(1)}, bf16[1,32,2048]{2,1,0:T(8,128)(2,1)S(1)}, u32[]{:S(2)}, u32[]{:S(2)}) %collective-permute-start.33) | collective-permute-done | bytes 131104 | tf_op jit(solution)/shard_map/ppermute | solution.py:34
  163.5 2.1 %collective-permute-start.34 = (bf16[32,2048]{1,0:T(8,128)(2,1)S(1)}, bf16[32,2048]{1,0:T(8,128)(2,1)S(1)}, u32[]{:S(2)}, u32[]{:S(2)}) collective-permute-start(bf16[32,2048]{1,0:T(8,128)(2,1)S(1)} %fusion.25), channel_id=1, source_target_pairs={{0,12},{4,0},{8,4},{12,8},{1,13},{5,1},{9,5},{13,9},{2,14},{6,2},{... | collective-permute-start | bytes 393224 | tf_op jit(solution)/shard_map/ppermute | solution.py:24
  166.3 1.2 collective-permute-start.37
  168.4 1.2 collective-permute-done.31
  169.5 1.6 collective-permute-done.34
  171.1 2.1 %collective-permute-done.37 = bf16[32,2048]{1,0:T(8,128)(2,1)S(1)} collective-permute-done((bf16[32,2048]{1,0:T(8,128)(2,1)S(1)}, bf16[32,2048]{1,0:T(8,128)(2,1)S(1)}, u32[]{:S(2)}, u32[]{:S(2)}) %collective-permute-start.37) | collective-permute-done | bytes 131104 | tf_op jit(solution)/shard_map/ppermute | solution.py:24
  174.3 4.4 %collective-permute-done.41 = bf16[32,2048]{1,0:T(8,128)(2,1)S(1)} collective-permute-done((bf16[32,2048]{1,0:T(8,128)(2,1)S(1)}, bf16[32,2048]{1,0:T(8,128)(2,1)S(1)}, u32[]{:S(2)}, u32[]{:S(2)}) %collective-permute-start.41) | collective-permute-done | bytes 131104 | tf_op jit(solution)/shard_map/ppermute | solution.py:34
  178.8 1.3 collective-permute-done.42
  (143 shorter events, 25.0 us)
Async XLA Ops:
  0.0 23.7 %copy-start = (bf16[256,2048]{1,0:T(8,128)(2,1)S(1)}, bf16[256,2048]{1,0:T(8,128)(2,1)}, u32[]{:S(2)}) copy-start(bf16[256,2048]{1,0:T(8,128)(2,1)} %param.17) | copy-start | bytes 3145732
  3.1 10.8 %collective-permute-start = (bf16[144,512]{1,0:T(8,128)(2,1)}, bf16[144,512]{1,0:T(8,128)(2,1)S(1)}, u32[]{:S(2)}, u32[]{:S(2)}) collective-permute-start(bf16[144,512]{1,0:T(8,128)(2,1)} %shard_map.118.refs_0_), channel_id=1, source_target_pairs={{0,4},{4,8},{8,12},{1,5},{5,9},{9,13},{2,6},{6,10},{10,14},{3,7},{... | collective-permute-start | bytes 442376 | tf_op jit(solution)/shard_map/ppermute | solution.py:29
  8.1 9.0 %collective-permute-start.1 = (bf16[144,512]{1,0:T(8,128)(2,1)}, bf16[144,512]{1,0:T(8,128)(2,1)S(1)}, u32[]{:S(2)}, u32[]{:S(2)}) collective-permute-start(bf16[144,512]{1,0:T(8,128)(2,1)} %shard_map.118.refs_0_), channel_id=1, source_target_pairs={{0,8},{4,12},{1,9},{5,13},{2,10},{6,14},{3,11},{7,15},{16,24},{20,... | collective-permute-start | bytes 442376 | tf_op jit(solution)/shard_map/ppermute | solution.py:29
  12.6 6.3 %collective-permute-start.2 = (bf16[144,512]{1,0:T(8,128)(2,1)}, bf16[144,512]{1,0:T(8,128)(2,1)S(1)}, u32[]{:S(2)}, u32[]{:S(2)}) collective-permute-start(bf16[144,512]{1,0:T(8,128)(2,1)} %shard_map.118.refs_0_), channel_id=1, source_target_pairs={{0,12},{1,13},{2,14},{3,15},{16,28},{17,29},{18,30},{19,31}} | collective-permute-start | bytes 442376 | tf_op jit(solution)/shard_map/ppermute | solution.py:29
  24.9 15.2 %collective-permute-start.3 = (bf16[32,2048]{1,0:T(8,128)(2,1)S(1)}, bf16[32,2048]{1,0:T(8,128)(2,1)S(1)}, u32[]{:S(2)}, u32[]{:S(2)}) collective-permute-start(bf16[32,2048]{1,0:T(8,128)(2,1)S(1)} %get-tuple-element.49), channel_id=1, source_target_pairs={{0,1},{1,0},{2,3},{3,2},{4,5},{5,4},{6,7},{7,6},{8,9},{9,8},{10,11... | collective-permute-start | bytes 393224 | tf_op jit(solution)/shard_map/ppermute | solution.py:34
  25.0 15.7 %collective-permute-start.4 = (bf16[32,2048]{1,0:T(8,128)(2,1)S(1)}, bf16[32,2048]{1,0:T(8,128)(2,1)S(1)}, u32[]{:S(2)}, u32[]{:S(2)}) collective-permute-start(bf16[32,2048]{1,0:T(8,128)(2,1)S(1)} %get-tuple-element.51), channel_id=1, source_target_pairs={{0,2},{1,3},{2,0},{3,1},{4,6},{5,7},{6,4},{7,5},{8,10},{9,11},{10,... | collective-permute-start | bytes 393224 | tf_op jit(solution)/shard_map/ppermute | solution.py:34
  26.5 16.5 %collective-permute-start.5 = (bf16[32,2048]{1,0:T(8,128)(2,1)S(1)}, bf16[32,2048]{1,0:T(8,128)(2,1)S(1)}, u32[]{:S(2)}, u32[]{:S(2)}) collective-permute-start(bf16[32,2048]{1,0:T(8,128)(2,1)S(1)} %get-tuple-element.50), channel_id=1, source_target_pairs={{0,3},{1,2},{2,1},{3,0},{4,7},{5,6},{6,5},{7,4},{8,11},{9,10},{10,... | collective-permute-start | bytes 393224 | tf_op jit(solution)/shard_map/ppermute | solution.py:34
  30.1 68.7 %collective-permute-start.21 = (bf16[384,640]{1,0:T(8,128)(2,1)}, bf16[384,640]{1,0:T(8,128)(2,1)S(1)}, u32[]{:S(2)}, u32[]{:S(2)}) collective-permute-start(bf16[384,640]{1,0:T(8,128)(2,1)} %get-tuple-element.26), channel_id=1, source_target_pairs={{0,4},{4,8},{8,12},{12,0},{1,5},{5,9},{9,13},{13,1},{2,6},{6,10},{... | collective-permute-start | bytes 1474568 | tf_op jit(solution)/shard_map/ppermute | solution.py:24
  34.3 10.1 %copy-start.35 = (f32[2048]{0:T(1024)S(1)}, f32[2048]{0:T(1024)}, u32[]{:S(2)}) copy-start(f32[2048]{0:T(1024)} %param.19) | copy-start | bytes 24580
  34.3 66.0 %collective-permute-start.25 = (bf16[384,640]{1,0:T(8,128)(2,1)}, bf16[384,640]{1,0:T(8,128)(2,1)S(1)}, u32[]{:S(2)}, u32[]{:S(2)}) collective-permute-start(bf16[384,640]{1,0:T(8,128)(2,1)} %get-tuple-element.28), channel_id=1, source_target_pairs={{0,12},{4,0},{8,4},{12,8},{1,13},{5,1},{9,5},{13,9},{2,14},{6,2},{... | collective-permute-start | bytes 1474568 | tf_op jit(solution)/shard_map/ppermute | solution.py:24
  40.1 46.2 %collective-permute-start.23 = (bf16[256,640]{1,0:T(8,128)(2,1)}, bf16[256,640]{1,0:T(8,128)(2,1)S(1)}, u32[]{:S(2)}, u32[]{:S(2)}) collective-permute-start(bf16[256,640]{1,0:T(8,128)(2,1)} %get-tuple-element.27), channel_id=1, source_target_pairs={{0,8},{4,12},{8,0},{12,4},{1,9},{5,13},{9,1},{13,5},{2,10},{6,14},... | collective-permute-start | bytes 983048 | tf_op jit(solution)/shard_map/ppermute | solution.py:24
  40.7 45.7 %collective-permute-start.27 = (bf16[128,640]{1,0:T(8,128)(2,1)}, bf16[128,640]{1,0:T(8,128)(2,1)}, u32[]{:S(2)}, u32[]{:S(2)}) collective-permute-start(bf16[128,640]{1,0:T(8,128)(2,1)} %get-tuple-element.32), channel_id=1, source_target_pairs={{0,8},{4,12},{8,0},{12,4},{1,9},{5,13},{9,1},{13,5},{2,10},{6,14},... | collective-permute-start | bytes 491528 | tf_op jit(solution)/shard_map/ppermute | solution.py:24
  44.4 54.4 %copy-start.27 = (bf16[32,2048]{1,0:T(8,128)(2,1)}, bf16[32,2048]{1,0:T(8,128)(2,1)S(1)}, u32[]{:S(2)}) copy-start(bf16[32,2048]{1,0:T(8,128)(2,1)S(1)} %get-tuple-element.46) | copy-start | bytes 393220
  44.5 41.8 %collective-permute-start.7 = (bf16[32,2048]{1,0:T(8,128)(2,1)S(1)}, bf16[32,2048]{1,0:T(8,128)(2,1)S(1)}, u32[]{:S(2)}, u32[]{:S(2)}) collective-permute-start(bf16[32,2048]{1,0:T(8,128)(2,1)S(1)} %fusion.8.refs_0_), channel_id=1, source_target_pairs={{0,4},{4,8},{8,12},{12,0},{1,5},{5,9},{9,13},{13,1},{2,6},{6,10},{... | collective-permute-start | bytes 393224 | tf_op jit(solution)/shard_map/ppermute | solution.py:24
  86.3 7.3 %collective-permute-start.9 = (bf16[32,2048]{1,0:T(8,128)(2,1)S(1)}, bf16[32,2048]{1,0:T(8,128)(2,1)S(1)}, u32[]{:S(2)}, u32[]{:S(2)}) collective-permute-start(bf16[32,2048]{1,0:T(8,128)(2,1)S(1)} %fusion.8.refs_0_), channel_id=1, source_target_pairs={{0,8},{4,12},{8,0},{12,4},{1,9},{5,13},{9,1},{13,5},{2,10},{6,14},... | collective-permute-start | bytes 393224 | tf_op jit(solution)/shard_map/ppermute | solution.py:24
  86.3 8.3 %collective-permute-start.11 = (bf16[32,2048]{1,0:T(8,128)(2,1)S(1)}, bf16[32,2048]{1,0:T(8,128)(2,1)S(1)}, u32[]{:S(2)}, u32[]{:S(2)}) collective-permute-start(bf16[32,2048]{1,0:T(8,128)(2,1)S(1)} %fusion.8.refs_0_), channel_id=1, source_target_pairs={{0,12},{4,0},{8,4},{12,8},{1,13},{5,1},{9,5},{13,9},{2,14},{6,2},{... | collective-permute-start | bytes 393224 | tf_op jit(solution)/shard_map/ppermute | solution.py:24
  86.3 9.7 %collective-permute-start.6 = (bf16[32,2048]{1,0:T(8,128)(2,1)S(1)}, bf16[32,2048]{1,0:T(8,128)(2,1)S(1)}, u32[]{:S(2)}, u32[]{:S(2)}) collective-permute-start(bf16[32,2048]{1,0:T(8,128)(2,1)S(1)} %fusion.8.refs_0_), channel_id=1, source_target_pairs={{0,2},{1,3},{2,0},{3,1},{4,6},{5,7},{6,4},{7,5},{8,10},{9,11},{10,... | collective-permute-start | bytes 393224 | tf_op jit(solution)/shard_map/ppermute | solution.py:34
  93.6 3.0 %collective-permute-start.13 = (bf16[32,2048]{1,0:T(8,128)(2,1)S(1)}, bf16[32,2048]{1,0:T(8,128)(2,1)S(1)}, u32[]{:S(2)}, u32[]{:S(2)}) collective-permute-start(bf16[32,2048]{1,0:T(8,128)(2,1)S(1)} %fusion.8.refs_0_), channel_id=1, source_target_pairs={{0,1},{1,0},{2,3},{3,2},{4,5},{5,4},{6,7},{7,6},{8,9},{9,8},{10,11... | collective-permute-start | bytes 393224 | tf_op jit(solution)/shard_map/ppermute | solution.py:34
  94.6 6.4 %collective-permute-start.8 = (bf16[32,2048]{1,0:T(8,128)(2,1)S(1)}, bf16[32,2048]{1,0:T(8,128)(2,1)S(1)}, u32[]{:S(2)}, u32[]{:S(2)}) collective-permute-start(bf16[32,2048]{1,0:T(8,128)(2,1)S(1)} %collective-permute-done.7.refs_2_), channel_id=1, source_target_pairs={{0,2},{1,3},{2,0},{3,1},{4,6},{5,7},{6,4},{7,5},{8,10},{9,11},{10,... | collective-permute-start | bytes 393224 | tf_op jit(solution)/shard_map/ppermute | solution.py:34
  96.1 7.8 %collective-permute-start.10 = (bf16[32,2048]{1,0:T(8,128)(2,1)S(1)}, bf16[32,2048]{1,0:T(8,128)(2,1)}, u32[]{:S(2)}, u32[]{:S(2)}) collective-permute-start(bf16[32,2048]{1,0:T(8,128)(2,1)S(1)} %collective-permute-done.9.refs_4_), channel_id=1, source_target_pairs={{0,2},{1,3},{2,0},{3,1},{4,6},{5,7},{6,4},{7,5},{8,10},{9,11},{10,... | collective-permute-start | bytes 393224 | tf_op jit(solution)/shard_map/ppermute | solution.py:34
  97.3 8.0 %collective-permute-start.12 = (bf16[32,2048]{1,0:T(8,128)(2,1)S(1)}, bf16[32,2048]{1,0:T(8,128)(2,1)}, u32[]{:S(2)}, u32[]{:S(2)}) collective-permute-start(bf16[32,2048]{1,0:T(8,128)(2,1)S(1)} %collective-permute-done.11.refs_6_), channel_id=1, source_target_pairs={{0,2},{1,3},{2,0},{3,1},{4,6},{5,7},{6,4},{7,5},{8,10},{9,11},{10,... | collective-permute-start | bytes 393224 | tf_op jit(solution)/shard_map/ppermute | solution.py:34
  98.8 35.6 %collective-permute-start.22 = (bf16[384,640]{1,0:T(8,128)(2,1)S(1)}, bf16[384,640]{1,0:T(8,128)(2,1)S(1)}, u32[]{:S(2)}, u32[]{:S(2)}) collective-permute-start(bf16[384,640]{1,0:T(8,128)(2,1)S(1)} %collective-permute-done.21.refs_17_.refs_0_), channel_id=1, source_target_pairs={{0,16},{16,0},{1,17},{17,1},{2,18},{18,2},{3,19},{19,3},{4,20},{20... | collective-permute-start | bytes 1474568 | tf_op jit(solution)/shard_map/ppermute | solution.py:24
  100.3 34.1 %collective-permute-start.26 = (bf16[384,640]{1,0:T(8,128)(2,1)S(1)}, bf16[384,640]{1,0:T(8,128)(2,1)S(1)}, u32[]{:S(2)}, u32[]{:S(2)}) collective-permute-start(bf16[384,640]{1,0:T(8,128)(2,1)S(1)} %collective-permute-done.25.refs_21_.refs_4_), channel_id=1, source_target_pairs={{0,16},{16,0},{1,17},{17,1},{2,18},{18,2},{3,19},{19,3},{4,20},{20... | collective-permute-start | bytes 1474568 | tf_op jit(solution)/shard_map/ppermute | solution.py:24
  101.0 27.2 %collective-permute-start.24 = (bf16[256,640]{1,0:T(8,128)(2,1)S(1)}, bf16[256,640]{1,0:T(8,128)(2,1)S(1)}, u32[]{:S(2)}, u32[]{:S(2)}) collective-permute-start(bf16[256,640]{1,0:T(8,128)(2,1)S(1)} %collective-permute-done.23.refs_19_), channel_id=1, source_target_pairs={{0,16},{16,0},{1,17},{17,1},{2,18},{18,2},{3,19},{19,3},{4,20},{20... | collective-permute-start | bytes 983048 | tf_op jit(solution)/shard_map/ppermute | solution.py:24
  103.9 2.1 %collective-permute-start.14 = (bf16[32,2048]{1,0:T(8,128)(2,1)S(1)}, bf16[32,2048]{1,0:T(8,128)(2,1)S(1)}, u32[]{:S(2)}, u32[]{:S(2)}) collective-permute-start(bf16[32,2048]{1,0:T(8,128)(2,1)S(1)} %collective-permute-done.6.refs_1_), channel_id=1, source_target_pairs={{0,1},{1,0},{2,3},{3,2},{4,5},{5,4},{6,7},{7,6},{8,9},{9,8},{10,11... | collective-permute-start | bytes 393224 | tf_op jit(solution)/shard_map/ppermute | solution.py:34
  105.3 2.5 %collective-permute-start.15 = (bf16[32,2048]{1,0:T(8,128)(2,1)S(1)}, bf16[32,2048]{1,0:T(8,128)(2,1)S(1)}, u32[]{:S(2)}, u32[]{:S(2)}) collective-permute-start(bf16[32,2048]{1,0:T(8,128)(2,1)S(1)} %collective-permute-done.7.refs_2_), channel_id=1, source_target_pairs={{0,1},{1,0},{2,3},{3,2},{4,5},{5,4},{6,7},{7,6},{8,9},{9,8},{10,11... | collective-permute-start | bytes 393224 | tf_op jit(solution)/shard_map/ppermute | solution.py:34
  106.6 2.5 %collective-permute-start.17 = (bf16[32,2048]{1,0:T(8,128)(2,1)S(1)}, bf16[32,2048]{1,0:T(8,128)(2,1)S(1)}, u32[]{:S(2)}, u32[]{:S(2)}) collective-permute-start(bf16[32,2048]{1,0:T(8,128)(2,1)S(1)} %collective-permute-done.9.refs_4_), channel_id=1, source_target_pairs={{0,1},{1,0},{2,3},{3,2},{4,5},{5,4},{6,7},{7,6},{8,9},{9,8},{10,11... | collective-permute-start | bytes 393224 | tf_op jit(solution)/shard_map/ppermute | solution.py:34
  108.4 2.5 %collective-permute-start.19 = (bf16[32,2048]{1,0:T(8,128)(2,1)S(1)}, bf16[32,2048]{1,0:T(8,128)(2,1)S(1)}, u32[]{:S(2)}, u32[]{:S(2)}) collective-permute-start(bf16[32,2048]{1,0:T(8,128)(2,1)S(1)} %collective-permute-done.11.refs_6_), channel_id=1, source_target_pairs={{0,1},{1,0},{2,3},{3,2},{4,5},{5,4},{6,7},{7,6},{8,9},{9,8},{10,11... | collective-permute-start | bytes 393224 | tf_op jit(solution)/shard_map/ppermute | solution.py:34
  109.7 19.2 %collective-permute-start.16 = (bf16[32,2048]{1,0:T(8,128)(2,1)S(1)}, bf16[32,2048]{1,0:T(8,128)(2,1)S(1)}, u32[]{:S(2)}, u32[]{:S(2)}) collective-permute-start(bf16[32,2048]{1,0:T(8,128)(2,1)S(1)} %collective-permute-done.8.refs_3_), channel_id=1, source_target_pairs={{0,1},{1,0},{2,3},{3,2},{4,5},{5,4},{6,7},{7,6},{8,9},{9,8},{10,11... | collective-permute-start | bytes 393224 | tf_op jit(solution)/shard_map/ppermute | solution.py:34
  111.5 22.8 %collective-permute-start.18 = (bf16[32,2048]{1,0:T(8,128)(2,1)}, bf16[32,2048]{1,0:T(8,128)(2,1)}, u32[]{:S(2)}, u32[]{:S(2)}) collective-permute-start(bf16[32,2048]{1,0:T(8,128)(2,1)} %collective-permute-done.10.refs_5_), channel_id=1, source_target_pairs={{0,1},{1,0},{2,3},{3,2},{4,5},{5,4},{6,7},{7,6},{8,9},{9,8},{10,11... | collective-permute-start | bytes 393224 | tf_op jit(solution)/shard_map/ppermute | solution.py:34
  128.9 5.4 %collective-permute-start.20 = (bf16[32,2048]{1,0:T(8,128)(2,1)}, bf16[32,2048]{1,0:T(8,128)(2,1)}, u32[]{:S(2)}, u32[]{:S(2)}) collective-permute-start(bf16[32,2048]{1,0:T(8,128)(2,1)} %collective-permute-done.12.refs_7_), channel_id=1, source_target_pairs={{0,1},{1,0},{2,3},{3,2},{4,5},{5,4},{6,7},{7,6},{8,9},{9,8},{10,11... | collective-permute-start | bytes 393224 | tf_op jit(solution)/shard_map/ppermute | solution.py:34
  129.6 20.5 %collective-permute-start.28 = (bf16[128,640]{1,0:T(8,128)(2,1)}, bf16[128,640]{1,0:T(8,128)(2,1)}, u32[]{:S(2)}, u32[]{:S(2)}) collective-permute-start(bf16[128,640]{1,0:T(8,128)(2,1)} %collective-permute-done.27.refs_2_), channel_id=1, source_target_pairs={{0,16},{16,0},{1,17},{17,1},{2,18},{18,2},{3,19},{19,3},{4,20},{20... | collective-permute-start | bytes 491528 | tf_op jit(solution)/shard_map/ppermute | solution.py:24
  152.6 1.6 collective-permute-start.29
  152.8 2.0 %collective-permute-start.32 = (bf16[64,2048]{1,0:T(8,128)(2,1)S(1)}, bf16[64,2048]{1,0:T(8,128)(2,1)S(1)}, u32[]{:S(2)}, u32[]{:S(2)}) collective-permute-start(bf16[64,2048]{1,0:T(8,128)(2,1)S(1)} %get-tuple-element.36), channel_id=1, source_target_pairs={{0,1},{1,0},{2,3},{3,2},{4,5},{5,4},{6,7},{7,6},{8,9},{9,8},{10,11... | collective-permute-start | bytes 786440 | tf_op jit(solution)/shard_map/ppermute | solution.py:34
  153.1 3.4 %collective-permute-start.35 = (bf16[64,2048]{1,0:T(8,128)(2,1)S(1)}, bf16[64,2048]{1,0:T(8,128)(2,1)S(1)}, u32[]{:S(2)}, u32[]{:S(2)}) collective-permute-start(bf16[64,2048]{1,0:T(8,128)(2,1)S(1)} %get-tuple-element.38), channel_id=1, source_target_pairs={{0,1},{1,0},{2,3},{3,2},{4,5},{5,4},{6,7},{7,6},{8,9},{9,8},{10,11... | collective-permute-start | bytes 786440 | tf_op jit(solution)/shard_map/ppermute | solution.py:34
  153.4 3.8 %collective-permute-start.38 = (bf16[64,2048]{1,0:T(8,128)(2,1)S(1)}, bf16[64,2048]{1,0:T(8,128)(2,1)S(1)}, u32[]{:S(2)}, u32[]{:S(2)}) collective-permute-start(bf16[64,2048]{1,0:T(8,128)(2,1)S(1)} %get-tuple-element.40), channel_id=1, source_target_pairs={{0,1},{1,0},{2,3},{3,2},{4,5},{5,4},{6,7},{7,6},{8,9},{9,8},{10,11... | collective-permute-start | bytes 786440 | tf_op jit(solution)/shard_map/ppermute | solution.py:34
  154.2 6.4 %collective-permute-start.30 = (bf16[1,32,2048]{2,1,0:T(8,128)(2,1)S(1)}, bf16[1,32,2048]{2,1,0:T(8,128)(2,1)S(1)}, u32[]{:S(2)}, u32[]{:S(2)}) collective-permute-start(bf16[1,32,2048]{2,1,0:T(8,128)(2,1)S(1)} %fusion.24), channel_id=1, source_target_pairs={{0,2},{1,3},{2,0},{3,1},{4,6},{5,7},{6,4},{7,5},{8,10},{9,11},{10,... | collective-permute-start | bytes 393224 | tf_op jit(solution)/shard_map/ppermute | solution.py:34
  154.9 8.6 %collective-permute-start.33 = (bf16[1,32,2048]{2,1,0:T(8,128)(2,1)S(1)}, bf16[1,32,2048]{2,1,0:T(8,128)(2,1)S(1)}, u32[]{:S(2)}, u32[]{:S(2)}) collective-permute-start(bf16[1,32,2048]{2,1,0:T(8,128)(2,1)S(1)} %fusion.26), channel_id=1, source_target_pairs={{0,2},{1,3},{2,0},{3,1},{4,6},{5,7},{6,4},{7,5},{8,10},{9,11},{10,... | collective-permute-start | bytes 393224 | tf_op jit(solution)/shard_map/ppermute | solution.py:34
  156.6 9.7 %collective-permute-start.36 = (bf16[1,32,2048]{2,1,0:T(8,128)(2,1)S(1)}, bf16[1,32,2048]{2,1,0:T(8,128)(2,1)S(1)}, u32[]{:S(2)}, u32[]{:S(2)}) collective-permute-start(bf16[1,32,2048]{2,1,0:T(8,128)(2,1)S(1)} %fusion.28), channel_id=1, source_target_pairs={{0,2},{1,3},{2,0},{3,1},{4,6},{5,7},{6,4},{7,5},{8,10},{9,11},{10,... | collective-permute-start | bytes 393224 | tf_op jit(solution)/shard_map/ppermute | solution.py:34
  157.3 11.1 %collective-permute-start.39 = (bf16[1,32,2048]{2,1,0:T(8,128)(2,1)S(1)}, bf16[1,32,2048]{2,1,0:T(8,128)(2,1)S(1)}, u32[]{:S(2)}, u32[]{:S(2)}) collective-permute-start(bf16[1,32,2048]{2,1,0:T(8,128)(2,1)S(1)} %fusion.29), channel_id=1, source_target_pairs={{0,2},{1,3},{2,0},{3,1},{4,6},{5,7},{6,4},{7,5},{8,10},{9,11},{10,... | collective-permute-start | bytes 393224 | tf_op jit(solution)/shard_map/ppermute | solution.py:34
  160.7 12.8 %copy-start.28 = (bf16[32,2048]{1,0:T(8,128)(2,1)S(1)}, bf16[32,2048]{1,0:T(8,128)(2,1)}, u32[]{:S(2)}) copy-start(bf16[32,2048]{1,0:T(8,128)(2,1)} %copy-done.27) | copy-start | bytes 393220
  160.7 12.8 %copy-start.33 = (f32[2048]{0:T(1024)S(1)}, f32[2048]{0:T(1024)}, u32[]{:S(2)}) copy-start(f32[2048]{0:T(1024)} %param.20) | copy-start | bytes 24580
  160.7 8.8 %collective-permute-start.31 = (bf16[32,2048]{1,0:T(8,128)(2,1)S(1)}, bf16[32,2048]{1,0:T(8,128)(2,1)S(1)}, u32[]{:S(2)}, u32[]{:S(2)}) collective-permute-start(bf16[32,2048]{1,0:T(8,128)(2,1)S(1)} %fusion.23), channel_id=1, source_target_pairs={{0,8},{4,12},{8,0},{12,4},{1,9},{5,13},{9,1},{13,5},{2,10},{6,14},... | collective-permute-start | bytes 393224 | tf_op jit(solution)/shard_map/ppermute | solution.py:24
  163.5 7.6 %collective-permute-start.34 = (bf16[32,2048]{1,0:T(8,128)(2,1)S(1)}, bf16[32,2048]{1,0:T(8,128)(2,1)S(1)}, u32[]{:S(2)}, u32[]{:S(2)}) collective-permute-start(bf16[32,2048]{1,0:T(8,128)(2,1)S(1)} %fusion.25), channel_id=1, source_target_pairs={{0,12},{4,0},{8,4},{12,8},{1,13},{5,1},{9,5},{13,9},{2,14},{6,2},{... | collective-permute-start | bytes 393224 | tf_op jit(solution)/shard_map/ppermute | solution.py:24
  166.3 6.9 %collective-permute-start.37 = (bf16[32,2048]{1,0:T(8,128)(2,1)S(1)}, bf16[32,2048]{1,0:T(8,128)(2,1)S(1)}, u32[]{:S(2)}, u32[]{:S(2)}) collective-permute-start(bf16[32,2048]{1,0:T(8,128)(2,1)S(1)} %fusion.27), channel_id=1, source_target_pairs={{0,4},{4,8},{8,12},{12,0},{1,5},{5,9},{9,13},{13,1},{2,6},{6,10},{... | collective-permute-start | bytes 393224 | tf_op jit(solution)/shard_map/ppermute | solution.py:24
  173.7 5.0 %collective-permute-start.41 = (bf16[32,2048]{1,0:T(8,128)(2,1)S(1)}, bf16[32,2048]{1,0:T(8,128)(2,1)S(1)}, u32[]{:S(2)}, u32[]{:S(2)}) collective-permute-start(bf16[32,2048]{1,0:T(8,128)(2,1)S(1)} %get-tuple-element.42), channel_id=1, source_target_pairs={{0,2},{1,3},{2,0},{3,1},{4,6},{5,7},{6,4},{7,5},{8,10},{9,11},{10,... | collective-permute-start | bytes 393224 | tf_op jit(solution)/shard_map/ppermute | solution.py:34
  174.3 4.4 %collective-permute-start.40 = (bf16[32,2048]{1,0:T(8,128)(2,1)S(1)}, bf16[32,2048]{1,0:T(8,128)(2,1)S(1)}, u32[]{:S(2)}, u32[]{:S(2)}) collective-permute-start(bf16[32,2048]{1,0:T(8,128)(2,1)S(1)} %get-tuple-element.42), channel_id=1, source_target_pairs={{0,1},{1,0},{2,3},{3,2},{4,5},{5,4},{6,7},{7,6},{8,9},{9,8},{10,11... | collective-permute-start | bytes 393224 | tf_op jit(solution)/shard_map/ppermute | solution.py:34
  178.7 1.3 collective-permute-start.42
  (31 other events, 41.4 us)

commit v2 on v1

--- a/solution.py
+++ b/solution.py
@@ -1,4 +1,5 @@
 import functools
+import math
 
 import jax
 import jax.numpy as jnp
@@ -10,7 +11,7 @@
 
 epsilon = 1e-06
 lanes = 128
-pad_rows = 16
+pad_rows = 8
 
 
 def normalize(payload_table):
@@ -34,11 +35,12 @@
     return lax.ppermute(rows, axis, [(i, i ^ bit) for i in range(count)])
 
 
-def call(kernel, outs, flops, *args, scratch=(), limit=None):
+def call(kernel, outs, flops, *args, scratch=(), limit=None, outside=0):
+    held = [pltpu.with_memory_space_constraint(arg, pltpu.VMEM) for arg in args[outside:]]
     specs = [pl.BlockSpec(memory_space=pltpu.VMEM)] * len(args)
     single = not isinstance(outs, list)
     out_list = [outs] if single else outs
-    moved = sum(a.size * a.dtype.itemsize for a in (*args, *out_list))
+    moved = sum(math.prod(a.shape) * a.dtype.itemsize for a in (*args, *out_list))
     out_specs = [pl.BlockSpec(memory_space=pltpu.VMEM)] * len(out_list)
     return pl.pallas_call(
         kernel,
@@ -48,7 +50,7 @@
         scratch_shapes=list(scratch),
         compiler_params=pltpu.CompilerParams(vmem_limit_bytes=limit),
         cost_estimate=pl.CostEstimate(flops=flops, bytes_accessed=moved, transcendentals=0),
-    )(*args)
+    )(*args[:outside], *held)
 
 
 def dot_t(a, b):
@@ -59,11 +61,9 @@
     tok_rows, width = key_ref.shape
     out_ref[:tok_rows, :width] = key_ref[...]
     out_ref[:tok_rows, width:] = value_ref[...]
-    head_count = logit_ref.shape[1]
-    row = lax.broadcasted_iota(jnp.int32, (pad_rows, head_count), 0)
-    column = lax.broadcasted_iota(jnp.int32, (pad_rows, head_count), 1)
-    pick = (row == column).astype(jnp.float32).astype(jnp.bfloat16)
-    out_ref[tok_rows:, :tok_rows] = dot_t(pick, logit_ref[...]).astype(out_ref.dtype)
+    logits = logit_ref[...].astype(jnp.float32)
+    rows = [logits, jnp.zeros((pad_rows - logits.shape[0], tok_rows), jnp.float32)]
+    out_ref[tok_rows:, :tok_rows] = jnp.concatenate(rows, axis=0).astype(out_ref.dtype)
     out_ref[tok_rows:, tok_rows:] = jnp.zeros((pad_rows, 2 * width - tok_rows), out_ref.dtype)
 
 
@@ -116,11 +116,12 @@
     ring = lax.axis_size("sp")
     packed = call(
         pack_kernel,
-        jax.ShapeDtypeStruct((tok_rows + pad_rows, 2 * width), key_part.dtype),
+        pltpu.VMEM((tok_rows + pad_rows, 2 * width), key_part.dtype),
         1,
         key_part,
         value_part,
-        logit_part,
+        jnp.transpose(logit_part),
+        outside=3,
     )
     blocks = [packed] + [upward(packed, "sp", step) for step in range(1, ring)]
     attended = call(
@@ -129,6 +130,7 @@
         10 * ring * tok_rows * tok_rows * width,
         queries,
         *blocks,
+        outside=1,
     )
     return attended, packed
 
@@ -249,7 +251,7 @@
             weight[pl.ds(start, share), :] = pieces[(step - 1) * copies + turn][:share]
     main = (own_ref.shape[1] - lanes) // 2
     count = rows_ref.shape[0]
-    tile = min(count, 256)
+    tile = min(count, 512)
 
     def body(index, _):
         rows = pl.ds(pl.multiple_of(index * tile, tile), tile)
@@ -336,8 +338,8 @@
         outer = [step for step in range(1, ring) if step != ring // 2]
 
         def pack(kernel, rows, *weights):
-            shapes = [jax.ShapeDtypeStruct((count, 2 * part), jnp.bfloat16) for count in rows]
-            return call(kernel, shapes, 1, *weights)
+            shapes = [pltpu.VMEM((count, 2 * part), jnp.bfloat16) for count in rows]
+            return call(kernel, shapes, 1, *weights, outside=len(weights))
 
         gate_in, up_in, _ = lax.optimization_barrier((gate_weight, up_weight, packed))
         pieces = pack(

time: 181 us -> 177 us (0.978)
  Pallas kernels: 21.4 us -> 17.7 us
  starting transfers between devices: 43.3 us -> 41.1 us
    pallas_call x7, Pallas kernels: 21.4 us -> 17.7 us  [call(): pl.pallas_call(kernel, out_shape=outs, in_specs=specs, out_specs=out_spec...]
    ppermute x14, starting transfers between devices: 18.5 us -> 16.4 us  [shift(): lax.ppermute(rows, axis, [(i, (i + step) % count) for i in range(count)])]
    unnamed x73 -> x76, local copies, waits for them, and re-layouts: 22.1 us -> 22.8 us
  transfers between devices with their start and end apart: 43 -> 43, of which waited for: 19 -> 19; matrix products, arithmetic and copies ran while one was open for 1% -> 2% of each run, Pallas kernels for 7% -> 6%
where the time goes in v2:
time: 177 us
  waiting for transfers between devices  88.8 us (50%)
  starting transfers between devices  41.1 us (23%)
  local copies, waits for them, and re-layouts  24.4 us (14%)
  Pallas kernels  17.7 us (10%)
  other arithmetic  3.18 us (2%)
    ppermute x14, waiting for transfers between devices, shift(): lax.ppermute(rows, axis, [(i, (i + step) % count) for i in range(count)])  68.6 us
    unnamed x76, local copies, waits for them, and re-layouts  22.8 us
    pallas_call x7, Pallas kernels, call(): pl.pallas_call(kernel, out_shape=outs, in_specs=specs, out_specs=out_spec...  17.7 us
    ppermute x14, starting transfers between devices, shift(): lax.ppermute(rows, axis, [(i, (i + step) % count) for i in range(count)])  16.4 us
    ppermute x26, waiting for transfers between devices, swap(): return lax.ppermute(rows, axis, [(i, i ^ bit) for i in range(count)])  15.9 us
    ppermute x26, starting transfers between devices, swap(): return lax.ppermute(rows, axis, [(i, i ^ bit) for i in range(count)])  14 us
    ppermute x3, starting transfers between devices, upward(): lax.ppermute(rows, axis, [(i, i + step) for i in range(count - step)])  10.8 us
    ppermute x3, waiting for transfers between devices, upward(): lax.ppermute(rows, axis, [(i, i + step) for i in range(count - step)])  4.32 us
  transfers between devices with their start and end apart: 43, of which 19 were waited for; matrix products, arithmetic and copies ran while one was open for 2% of the time, Pallas kernels for 6%

profile of v2, /device:TPU:0, one launch (start us, length us, event | category | flops | bytes accessed | tf_op | source)
XLA Modules:
  0.0 176.8 jit_solution(7101971185478167652)
XLA Ops:
  0.0 1.0 shard_map.118.refs_0_
  1.0 5.0 %collective-permute-start = (bf16[136,512]{1,0:T(8,128)(2,1)S(1)}, bf16[136,512]{1,0:T(8,128)(2,1)S(1)}, u32[]{:S(2)}, u32[]{:S(2)}) collective-permute-start(bf16[136,512]{1,0:T(8,128)(2,1)S(1)} %shard_map.118.refs_0_), channel_id=1, source_target_pairs={{0,4},{4,8},{8,12},{1,5},{5,9},{9,13},{2,6},{6,10},{10,14},{3,7},{... | collective-permute-start | bytes 417800 | tf_op jit(solution)/shard_map/ppermute | solution.py:30
  6.0 4.5 %collective-permute-start.1 = (bf16[136,512]{1,0:T(8,128)(2,1)S(1)}, bf16[136,512]{1,0:T(8,128)(2,1)S(1)}, u32[]{:S(2)}, u32[]{:S(2)}) collective-permute-start(bf16[136,512]{1,0:T(8,128)(2,1)S(1)} %shard_map.118.refs_0_), channel_id=1, source_target_pairs={{0,8},{4,12},{1,9},{5,13},{2,10},{6,14},{3,11},{7,15},{16,24},{20,... | collective-permute-start | bytes 417800 | tf_op jit(solution)/shard_map/ppermute | solution.py:30
  10.5 1.3 collective-permute-start.2
  11.8 2.7 %collective-permute-done.1.refs_2_ = bf16[136,512]{1,0:T(8,128)(2,1)S(1)} collective-permute-done((bf16[136,512]{1,0:T(8,128)(2,1)S(1)}, bf16[136,512]{1,0:T(8,128)(2,1)S(1)}, u32[]{:S(2)}, u32[]{:S(2)}) %collective-permute-start.1) | collective-permute-done | bytes 139296 | tf_op jit(solution)/shard_map/ppermute | solution.py:30
  14.5 1.6 collective-permute-done.2.refs_3_
  16.1 3.8 %shard_map.119 = bf16[128,256]{1,0:T(8,128)(2,1)} custom-call(bf16[128,256]{1,0:T(8,128)(2,1)} %query_ref.1, bf16[136,512]{1,0:T(8,128)(2,1)S(1)} %shard_map.118.refs_0_, bf16[136,512]{1,0:T(8,128)(2,1)S(1)} %collective-permute-done.refs_1_, bf16[136,512]{1,0:T(8,128)(2,1)S(1)} %collective-permute-done.1.refs_2_, ...), custom_call_target="tpu_custom_call" | custom-call | flops 167772160 | bytes 688128 | tf_op jit(solution)/shard_map/pallas_call | solution.py:45
  19.9 1.1 convolution_convert_fusion
  21.9 1.5 collective-permute-start.4
  23.8 2.3 %shard_map.121 = (bf16[384,640]{1,0:T(8,128)(2,1)S(1)}, bf16[384,640]{1,0:T(8,128)(2,1)S(1)}) custom-call(bf16[512,1280]{1,0:T(8,128)(2,1)} %gate_ref.4, bf16[512,1280]{1,0:T(8,128)(2,1)} %up_ref.4, bf16[512,1280]{1,0:T(8,128)(2,1)} %down_ref.5), custom_call_target="tpu_custom_call" | custom-call | flops 1 | bytes 4915200 | tf_op jit(solution)/shard_map/pallas_call | solution.py:45
  26.1 3.3 %collective-permute-start.21 = (bf16[384,640]{1,0:T(8,128)(2,1)S(1)}, bf16[384,640]{1,0:T(8,128)(2,1)S(1)}, u32[]{:S(2)}, u32[]{:S(2)}) collective-permute-start(bf16[384,640]{1,0:T(8,128)(2,1)S(1)} %get-tuple-element.26), channel_id=1, source_target_pairs={{0,4},{4,8},{8,12},{12,0},{1,5},{5,9},{9,13},{13,1},{2,6},{6,10},{... | collective-permute-start | bytes 1474568 | tf_op jit(solution)/shard_map/ppermute | solution.py:25
  29.4 2.9 %collective-permute-start.25 = (bf16[384,640]{1,0:T(8,128)(2,1)S(1)}, bf16[384,640]{1,0:T(8,128)(2,1)S(1)}, u32[]{:S(2)}, u32[]{:S(2)}) collective-permute-start(bf16[384,640]{1,0:T(8,128)(2,1)S(1)} %get-tuple-element.28), channel_id=1, source_target_pairs={{0,12},{4,0},{8,4},{12,8},{1,13},{5,1},{9,5},{13,9},{2,14},{6,2},{... | collective-permute-start | bytes 1474568 | tf_op jit(solution)/shard_map/ppermute | solution.py:25
  32.3 2.2 %shard_map.122 = (bf16[256,640]{1,0:T(8,128)(2,1)S(1)}, bf16[128,640]{1,0:T(8,128)(2,1)S(1)}) custom-call(bf16[512,1280]{1,0:T(8,128)(2,1)} %gate_ref.4, bf16[512,1280]{1,0:T(8,128)(2,1)} %up_ref.4, bf16[512,1280]{1,0:T(8,128)(2,1)} %down_ref.5), custom_call_target="tpu_custom_call" | custom-call | flops 1 | bytes 4423680 | tf_op jit(solution)/shard_map/pallas_call | solution.py:45
  35.2 2.4 %collective-permute-start.27 = (bf16[128,640]{1,0:T(8,128)(2,1)S(1)}, bf16[128,640]{1,0:T(8,128)(2,1)}, u32[]{:S(2)}, u32[]{:S(2)}) collective-permute-start(bf16[128,640]{1,0:T(8,128)(2,1)S(1)} %get-tuple-element.32), channel_id=1, source_target_pairs={{0,8},{4,12},{8,0},{12,4},{1,9},{5,13},{9,1},{13,5},{2,10},{6,14},... | collective-permute-start | bytes 491528 | tf_op jit(solution)/shard_map/ppermute | solution.py:25
  37.6 1.3 fusion
  38.9 1.2 fusion.6
  40.2 41.0 %collective-permute-done.27.refs_2_ = bf16[128,640]{1,0:T(8,128)(2,1)} collective-permute-done((bf16[128,640]{1,0:T(8,128)(2,1)S(1)}, bf16[128,640]{1,0:T(8,128)(2,1)}, u32[]{:S(2)}, u32[]{:S(2)}) %collective-permute-start.27) | collective-permute-done | bytes 163872 | tf_op jit(solution)/shard_map/ppermute | solution.py:25
  81.3 1.6 collective-permute-start.6
  82.8 5.7 %collective-permute-done.9.refs_4_ = bf16[32,2048]{1,0:T(8,128)(2,1)S(1)} collective-permute-done((bf16[32,2048]{1,0:T(8,128)(2,1)S(1)}, bf16[32,2048]{1,0:T(8,128)(2,1)S(1)}, u32[]{:S(2)}, u32[]{:S(2)}) %collective-permute-start.9) | collective-permute-done | bytes 131104 | tf_op jit(solution)/shard_map/ppermute | solution.py:25
  89.5 1.5 collective-permute-start.8
  92.2 1.5 collective-permute-start.12
  93.7 1.5 collective-permute-start.22
  95.9 1.5 collective-permute-start.24
  99.5 1.4 collective-permute-done.12.refs_7_
  107.1 16.6 %collective-permute-done.24.refs_20_ = bf16[256,640]{1,0:T(8,128)(2,1)S(1)} collective-permute-done((bf16[256,640]{1,0:T(8,128)(2,1)S(1)}, bf16[256,640]{1,0:T(8,128)(2,1)S(1)}, u32[]{:S(2)}, u32[]{:S(2)}) %collective-permute-start.24) | collective-permute-done | bytes 327712 | tf_op jit(solution)/shard_map/ppermute | solution.py:25
  125.1 1.5 collective-permute-start.28
  126.6 2.3 %shard_map.120 = (bf16[512,640]{1,0:T(8,128)(2,1)S(1)}, bf16[256,640]{1,0:T(8,128)(2,1)S(1)}) custom-call(bf16[512,1280]{1,0:T(8,128)(2,1)} %gate_ref.4, bf16[512,1280]{1,0:T(8,128)(2,1)} %up_ref.4, bf16[512,1280]{1,0:T(8,128)(2,1)} %down_ref.5), custom_call_target="tpu_custom_call" | custom-call | flops 1 | bytes 4915200 | tf_op jit(solution)/shard_map/pallas_call | solution.py:45
  130.6 1.0 copy-done.4
  131.6 1.0 copy-done.6
  132.6 0.9 copy-done.10
  133.5 0.9 copy-done.12
  134.4 0.9 copy-done.14
  135.3 0.9 copy-done.16
  137.1 0.9 copy-done.20
  142.5 3.5 %shard_map.123 = (bf16[512,384]{1,0:T(8,128)(2,1)S(1)}, bf16[512,384]{1,0:T(8,128)(2,1)S(1)}) custom-call(bf16[32,2048]{1,0:T(8,128)(2,1)S(1)} %copy-done.2, bf16[32,2048]{1,0:T(8,128)(2,1)S(1)} %copy-done.16, bf16[32,2048]{1,0:T(8,128)(2,1)S(1)} %copy-done.10, bf16[32,2048]{1,0:T(8,128)(2,1)S(1)} %copy-done.20, bf16[32,2048]{1,0:T(8,128)(2,1)S(1)} %copy-done.12, ...), custom_call_target="tpu_custom_call" | custom-call | flops 1342177280 | bytes 6160384 | tf_op jit(solution)/shard_map/pallas_call | solution.py:45
  146.0 2.6 %shard_map.124 = (bf16[64,2048]{1,0:T(8,128)(2,1)S(1)}, bf16[64,2048]{1,0:T(8,128)(2,1)S(1)}, bf16[64,2048]{1,0:T(8,128)(2,1)S(1)}, bf16[64,2048]{1,0:T(8,128)(2...) custom-call(bf16[512,384]{1,0:T(8,128)(2,1)S(1)} %get-tuple-element., ...), custom_call_target="tpu_custom_call" | custom-call | flops 671088640 | bytes 5505024 | tf_op jit(solution)/shard_map/pallas_call | solution.py:45
  151.0 1.6 collective-permute-start.33
  153.3 1.6 collective-permute-start.39
  154.9 1.9 %collective-permute-done.30 = bf16[1,32,2048]{2,1,0:T(8,128)(2,1)S(1)} collective-permute-done((bf16[1,32,2048]{2,1,0:T(8,128)(2,1)S(1)}, bf16[1,32,2048]{2,1,0:T(8,128)(2,1)S(1)}, u32[]{:S(2)}, u32[]{:S(2)}) %collective-permute-start.30) | collective-permute-done | bytes 131104 | tf_op jit(solution)/shard_map/ppermute | solution.py:35
  156.9 2.7 %collective-permute-done.33 = bf16[1,32,2048]{2,1,0:T(8,128)(2,1)S(1)} collective-permute-done((bf16[1,32,2048]{2,1,0:T(8,128)(2,1)S(1)}, bf16[1,32,2048]{2,1,0:T(8,128)(2,1)S(1)}, u32[]{:S(2)}, u32[]{:S(2)}) %collective-permute-start.33) | collective-permute-done | bytes 131104 | tf_op jit(solution)/shard_map/ppermute | solution.py:35
  159.6 1.4 collective-permute-start.34
  161.0 1.4 collective-permute-done.36
  162.9 1.5 collective-permute-done.39
  164.4 1.1 collective-permute-done.31
  165.5 1.8 %collective-permute-done.34 = bf16[32,2048]{1,0:T(8,128)(2,1)S(1)} collective-permute-done((bf16[32,2048]{1,0:T(8,128)(2,1)S(1)}, bf16[32,2048]{1,0:T(8,128)(2,1)S(1)}, u32[]{:S(2)}, u32[]{:S(2)}) %collective-permute-start.34) | collective-permute-done | bytes 131104 | tf_op jit(solution)/shard_map/ppermute | solution.py:25
  167.3 2.0 %collective-permute-done.37 = bf16[32,2048]{1,0:T(8,128)(2,1)S(1)} collective-permute-done((bf16[32,2048]{1,0:T(8,128)(2,1)S(1)}, bf16[32,2048]{1,0:T(8,128)(2,1)S(1)}, u32[]{:S(2)}, u32[]{:S(2)}) %collective-permute-start.37) | collective-permute-done | bytes 131104 | tf_op jit(solution)/shard_map/ppermute | solution.py:25
  170.3 4.4 %collective-permute-done.41 = bf16[32,2048]{1,0:T(8,128)(2,1)S(1)} collective-permute-done((bf16[32,2048]{1,0:T(8,128)(2,1)S(1)}, bf16[32,2048]{1,0:T(8,128)(2,1)S(1)}, u32[]{:S(2)}, u32[]{:S(2)}) %collective-permute-start.41) | collective-permute-done | bytes 131104 | tf_op jit(solution)/shard_map/ppermute | solution.py:35
  174.8 1.3 collective-permute-done.42
  (146 shorter events, 27.0 us)
Async XLA Ops:
  0.0 19.9 %copy-start = (bf16[256,2048]{1,0:T(8,128)(2,1)S(1)}, bf16[256,2048]{1,0:T(8,128)(2,1)}, u32[]{:S(2)}) copy-start(bf16[256,2048]{1,0:T(8,128)(2,1)} %param.17) | copy-start | bytes 3145732
  1.0 10.8 %collective-permute-start = (bf16[136,512]{1,0:T(8,128)(2,1)S(1)}, bf16[136,512]{1,0:T(8,128)(2,1)S(1)}, u32[]{:S(2)}, u32[]{:S(2)}) collective-permute-start(bf16[136,512]{1,0:T(8,128)(2,1)S(1)} %shard_map.118.refs_0_), channel_id=1, source_target_pairs={{0,4},{4,8},{8,12},{1,5},{5,9},{9,13},{2,6},{6,10},{10,14},{3,7},{... | collective-permute-start | bytes 417800 | tf_op jit(solution)/shard_map/ppermute | solution.py:30
  6.0 8.5 %collective-permute-start.1 = (bf16[136,512]{1,0:T(8,128)(2,1)S(1)}, bf16[136,512]{1,0:T(8,128)(2,1)S(1)}, u32[]{:S(2)}, u32[]{:S(2)}) collective-permute-start(bf16[136,512]{1,0:T(8,128)(2,1)S(1)} %shard_map.118.refs_0_), channel_id=1, source_target_pairs={{0,8},{4,12},{1,9},{5,13},{2,10},{6,14},{3,11},{7,15},{16,24},{20,... | collective-permute-start | bytes 417800 | tf_op jit(solution)/shard_map/ppermute | solution.py:30
  10.5 5.7 %collective-permute-start.2 = (bf16[136,512]{1,0:T(8,128)(2,1)S(1)}, bf16[136,512]{1,0:T(8,128)(2,1)S(1)}, u32[]{:S(2)}, u32[]{:S(2)}) collective-permute-start(bf16[136,512]{1,0:T(8,128)(2,1)S(1)} %shard_map.118.refs_0_), channel_id=1, source_target_pairs={{0,12},{1,13},{2,14},{3,15},{16,28},{17,29},{18,30},{19,31}} | collective-permute-start | bytes 417800 | tf_op jit(solution)/shard_map/ppermute | solution.py:30
  21.9 12.7 %collective-permute-start.3 = (bf16[32,2048]{1,0:T(8,128)(2,1)}, bf16[32,2048]{1,0:T(8,128)(2,1)}, u32[]{:S(2)}, u32[]{:S(2)}) collective-permute-start(bf16[32,2048]{1,0:T(8,128)(2,1)} %get-tuple-element.49), channel_id=1, source_target_pairs={{0,1},{1,0},{2,3},{3,2},{4,5},{5,4},{6,7},{7,6},{8,9},{9,8},{10,11... | collective-permute-start | bytes 393224 | tf_op jit(solution)/shard_map/ppermute | solution.py:35
  21.9 13.2 %collective-permute-start.4 = (bf16[32,2048]{1,0:T(8,128)(2,1)}, bf16[32,2048]{1,0:T(8,128)(2,1)}, u32[]{:S(2)}, u32[]{:S(2)}) collective-permute-start(bf16[32,2048]{1,0:T(8,128)(2,1)} %get-tuple-element.51), channel_id=1, source_target_pairs={{0,2},{1,3},{2,0},{3,1},{4,6},{5,7},{6,4},{7,5},{8,10},{9,11},{10,... | collective-permute-start | bytes 393224 | tf_op jit(solution)/shard_map/ppermute | solution.py:35
  23.4 14.2 %collective-permute-start.5 = (bf16[32,2048]{1,0:T(8,128)(2,1)}, bf16[32,2048]{1,0:T(8,128)(2,1)}, u32[]{:S(2)}, u32[]{:S(2)}) collective-permute-start(bf16[32,2048]{1,0:T(8,128)(2,1)} %get-tuple-element.50), channel_id=1, source_target_pairs={{0,3},{1,2},{2,1},{3,0},{4,7},{5,6},{6,5},{7,4},{8,11},{9,10},{10,... | collective-permute-start | bytes 393224 | tf_op jit(solution)/shard_map/ppermute | solution.py:35
  26.1 67.6 %collective-permute-start.21 = (bf16[384,640]{1,0:T(8,128)(2,1)S(1)}, bf16[384,640]{1,0:T(8,128)(2,1)S(1)}, u32[]{:S(2)}, u32[]{:S(2)}) collective-permute-start(bf16[384,640]{1,0:T(8,128)(2,1)S(1)} %get-tuple-element.26), channel_id=1, source_target_pairs={{0,4},{4,8},{8,12},{12,0},{1,5},{5,9},{9,13},{13,1},{2,6},{6,10},{... | collective-permute-start | bytes 1474568 | tf_op jit(solution)/shard_map/ppermute | solution.py:25
  29.4 10.6 %copy-start.37 = (f32[2048]{0:T(1024)S(1)}, f32[2048]{0:T(1024)}, u32[]{:S(2)}) copy-start(f32[2048]{0:T(1024)} %param.19) | copy-start | bytes 24580
  29.4 65.8 %collective-permute-start.25 = (bf16[384,640]{1,0:T(8,128)(2,1)S(1)}, bf16[384,640]{1,0:T(8,128)(2,1)S(1)}, u32[]{:S(2)}, u32[]{:S(2)}) collective-permute-start(bf16[384,640]{1,0:T(8,128)(2,1)S(1)} %get-tuple-element.28), channel_id=1, source_target_pairs={{0,12},{4,0},{8,4},{12,8},{1,13},{5,1},{9,5},{13,9},{2,14},{6,2},{... | collective-permute-start | bytes 1474568 | tf_op jit(solution)/shard_map/ppermute | solution.py:25
  34.6 46.6 %collective-permute-start.23 = (bf16[256,640]{1,0:T(8,128)(2,1)S(1)}, bf16[256,640]{1,0:T(8,128)(2,1)S(1)}, u32[]{:S(2)}, u32[]{:S(2)}) collective-permute-start(bf16[256,640]{1,0:T(8,128)(2,1)S(1)} %get-tuple-element.27), channel_id=1, source_target_pairs={{0,8},{4,12},{8,0},{12,4},{1,9},{5,13},{9,1},{13,5},{2,10},{6,14},... | collective-permute-start | bytes 983048 | tf_op jit(solution)/shard_map/ppermute | solution.py:25
  35.2 46.1 %collective-permute-start.27 = (bf16[128,640]{1,0:T(8,128)(2,1)S(1)}, bf16[128,640]{1,0:T(8,128)(2,1)}, u32[]{:S(2)}, u32[]{:S(2)}) collective-permute-start(bf16[128,640]{1,0:T(8,128)(2,1)S(1)} %get-tuple-element.32), channel_id=1, source_target_pairs={{0,8},{4,12},{8,0},{12,4},{1,9},{5,13},{9,1},{13,5},{2,10},{6,14},... | collective-permute-start | bytes 491528 | tf_op jit(solution)/shard_map/ppermute | solution.py:25
  40.0 84.4 %copy-start.32 = (bf16[32,2048]{1,0:T(8,128)(2,1)}, bf16[32,2048]{1,0:T(8,128)(2,1)S(1)}, u32[]{:S(2)}) copy-start(bf16[32,2048]{1,0:T(8,128)(2,1)S(1)} %get-tuple-element.46) | copy-start | bytes 393220
  40.2 41.1 %collective-permute-start.7 = (bf16[32,2048]{1,0:T(8,128)(2,1)S(1)}, bf16[32,2048]{1,0:T(8,128)(2,1)S(1)}, u32[]{:S(2)}, u32[]{:S(2)}) collective-permute-start(bf16[32,2048]{1,0:T(8,128)(2,1)S(1)} %fusion.8.refs_0_), channel_id=1, source_target_pairs={{0,4},{4,8},{8,12},{12,0},{1,5},{5,9},{9,13},{13,1},{2,6},{6,10},{... | collective-permute-start | bytes 393224 | tf_op jit(solution)/shard_map/ppermute | solution.py:25
  81.2 7.3 %collective-permute-start.9 = (bf16[32,2048]{1,0:T(8,128)(2,1)S(1)}, bf16[32,2048]{1,0:T(8,128)(2,1)S(1)}, u32[]{:S(2)}, u32[]{:S(2)}) collective-permute-start(bf16[32,2048]{1,0:T(8,128)(2,1)S(1)} %fusion.8.refs_0_), channel_id=1, source_target_pairs={{0,8},{4,12},{8,0},{12,4},{1,9},{5,13},{9,1},{13,5},{2,10},{6,14},... | collective-permute-start | bytes 393224 | tf_op jit(solution)/shard_map/ppermute | solution.py:25
  81.2 8.3 %collective-permute-start.11 = (bf16[32,2048]{1,0:T(8,128)(2,1)S(1)}, bf16[32,2048]{1,0:T(8,128)(2,1)S(1)}, u32[]{:S(2)}, u32[]{:S(2)}) collective-permute-start(bf16[32,2048]{1,0:T(8,128)(2,1)S(1)} %fusion.8.refs_0_), channel_id=1, source_target_pairs={{0,12},{4,0},{8,4},{12,8},{1,13},{5,1},{9,5},{13,9},{2,14},{6,2},{... | collective-permute-start | bytes 393224 | tf_op jit(solution)/shard_map/ppermute | solution.py:25
  81.3 9.7 %collective-permute-start.6 = (bf16[32,2048]{1,0:T(8,128)(2,1)S(1)}, bf16[32,2048]{1,0:T(8,128)(2,1)S(1)}, u32[]{:S(2)}, u32[]{:S(2)}) collective-permute-start(bf16[32,2048]{1,0:T(8,128)(2,1)S(1)} %fusion.8.refs_0_), channel_id=1, source_target_pairs={{0,2},{1,3},{2,0},{3,1},{4,6},{5,7},{6,4},{7,5},{8,10},{9,11},{10,... | collective-permute-start | bytes 393224 | tf_op jit(solution)/shard_map/ppermute | solution.py:35
  88.6 3.0 %collective-permute-start.13 = (bf16[32,2048]{1,0:T(8,128)(2,1)S(1)}, bf16[32,2048]{1,0:T(8,128)(2,1)S(1)}, u32[]{:S(2)}, u32[]{:S(2)}) collective-permute-start(bf16[32,2048]{1,0:T(8,128)(2,1)S(1)} %fusion.8.refs_0_), channel_id=1, source_target_pairs={{0,1},{1,0},{2,3},{3,2},{4,5},{5,4},{6,7},{7,6},{8,9},{9,8},{10,11... | collective-permute-start | bytes 393224 | tf_op jit(solution)/shard_map/ppermute | solution.py:35
  89.5 6.4 %collective-permute-start.8 = (bf16[32,2048]{1,0:T(8,128)(2,1)S(1)}, bf16[32,2048]{1,0:T(8,128)(2,1)S(1)}, u32[]{:S(2)}, u32[]{:S(2)}) collective-permute-start(bf16[32,2048]{1,0:T(8,128)(2,1)S(1)} %collective-permute-done.7.refs_2_), channel_id=1, source_target_pairs={{0,2},{1,3},{2,0},{3,1},{4,6},{5,7},{6,4},{7,5},{8,10},{9,11},{10,... | collective-permute-start | bytes 393224 | tf_op jit(solution)/shard_map/ppermute | solution.py:35
  91.0 7.8 %collective-permute-start.10 = (bf16[32,2048]{1,0:T(8,128)(2,1)S(1)}, bf16[32,2048]{1,0:T(8,128)(2,1)}, u32[]{:S(2)}, u32[]{:S(2)}) collective-permute-start(bf16[32,2048]{1,0:T(8,128)(2,1)S(1)} %collective-permute-done.9.refs_4_), channel_id=1, source_target_pairs={{0,2},{1,3},{2,0},{3,1},{4,6},{5,7},{6,4},{7,5},{8,10},{9,11},{10,... | collective-permute-start | bytes 393224 | tf_op jit(solution)/shard_map/ppermute | solution.py:35
  92.2 8.6 %collective-permute-start.12 = (bf16[32,2048]{1,0:T(8,128)(2,1)S(1)}, bf16[32,2048]{1,0:T(8,128)(2,1)}, u32[]{:S(2)}, u32[]{:S(2)}) collective-permute-start(bf16[32,2048]{1,0:T(8,128)(2,1)S(1)} %collective-permute-done.11.refs_6_), channel_id=1, source_target_pairs={{0,2},{1,3},{2,0},{3,1},{4,6},{5,7},{6,4},{7,5},{8,10},{9,11},{10,... | collective-permute-start | bytes 393224 | tf_op jit(solution)/shard_map/ppermute | solution.py:35
  93.7 36.0 %collective-permute-start.22 = (bf16[384,640]{1,0:T(8,128)(2,1)S(1)}, bf16[384,640]{1,0:T(8,128)(2,1)S(1)}, u32[]{:S(2)}, u32[]{:S(2)}) collective-permute-start(bf16[384,640]{1,0:T(8,128)(2,1)S(1)} %collective-permute-done.21.refs_17_.refs_0_), channel_id=1, source_target_pairs={{0,16},{16,0},{1,17},{17,1},{2,18},{18,2},{3,19},{19,3},{4,20},{20... | collective-permute-start | bytes 1474568 | tf_op jit(solution)/shard_map/ppermute | solution.py:25
  95.2 34.5 %collective-permute-start.26 = (bf16[384,640]{1,0:T(8,128)(2,1)S(1)}, bf16[384,640]{1,0:T(8,128)(2,1)}, u32[]{:S(2)}, u32[]{:S(2)}) collective-permute-start(bf16[384,640]{1,0:T(8,128)(2,1)S(1)} %collective-permute-done.25.refs_21_.refs_4_), channel_id=1, source_target_pairs={{0,16},{16,0},{1,17},{17,1},{2,18},{18,2},{3,19},{19,3},{4,20},{20... | collective-permute-start | bytes 1474568 | tf_op jit(solution)/shard_map/ppermute | solution.py:25
  95.9 27.9 %collective-permute-start.24 = (bf16[256,640]{1,0:T(8,128)(2,1)S(1)}, bf16[256,640]{1,0:T(8,128)(2,1)S(1)}, u32[]{:S(2)}, u32[]{:S(2)}) collective-permute-start(bf16[256,640]{1,0:T(8,128)(2,1)S(1)} %collective-permute-done.23.refs_19_), channel_id=1, source_target_pairs={{0,16},{16,0},{1,17},{17,1},{2,18},{18,2},{3,19},{19,3},{4,20},{20... | collective-permute-start | bytes 983048 | tf_op jit(solution)/shard_map/ppermute | solution.py:25
  98.8 2.7 %collective-permute-start.14 = (bf16[32,2048]{1,0:T(8,128)(2,1)S(1)}, bf16[32,2048]{1,0:T(8,128)(2,1)S(1)}, u32[]{:S(2)}, u32[]{:S(2)}) collective-permute-start(bf16[32,2048]{1,0:T(8,128)(2,1)S(1)} %collective-permute-done.6.refs_1_), channel_id=1, source_target_pairs={{0,1},{1,0},{2,3},{3,2},{4,5},{5,4},{6,7},{7,6},{8,9},{9,8},{10,11... | collective-permute-start | bytes 393224 | tf_op jit(solution)/shard_map/ppermute | solution.py:35
  100.8 2.5 %collective-permute-start.15 = (bf16[32,2048]{1,0:T(8,128)(2,1)S(1)}, bf16[32,2048]{1,0:T(8,128)(2,1)S(1)}, u32[]{:S(2)}, u32[]{:S(2)}) collective-permute-start(bf16[32,2048]{1,0:T(8,128)(2,1)S(1)} %collective-permute-done.7.refs_2_), channel_id=1, source_target_pairs={{0,1},{1,0},{2,3},{3,2},{4,5},{5,4},{6,7},{7,6},{8,9},{9,8},{10,11... | collective-permute-start | bytes 393224 | tf_op jit(solution)/shard_map/ppermute | solution.py:35
  102.2 2.5 %collective-permute-start.17 = (bf16[32,2048]{1,0:T(8,128)(2,1)S(1)}, bf16[32,2048]{1,0:T(8,128)(2,1)S(1)}, u32[]{:S(2)}, u32[]{:S(2)}) collective-permute-start(bf16[32,2048]{1,0:T(8,128)(2,1)S(1)} %collective-permute-done.9.refs_4_), channel_id=1, source_target_pairs={{0,1},{1,0},{2,3},{3,2},{4,5},{5,4},{6,7},{7,6},{8,9},{9,8},{10,11... | collective-permute-start | bytes 393224 | tf_op jit(solution)/shard_map/ppermute | solution.py:35
  104.0 2.5 %collective-permute-start.19 = (bf16[32,2048]{1,0:T(8,128)(2,1)S(1)}, bf16[32,2048]{1,0:T(8,128)(2,1)S(1)}, u32[]{:S(2)}, u32[]{:S(2)}) collective-permute-start(bf16[32,2048]{1,0:T(8,128)(2,1)S(1)} %collective-permute-done.11.refs_6_), channel_id=1, source_target_pairs={{0,1},{1,0},{2,3},{3,2},{4,5},{5,4},{6,7},{7,6},{8,9},{9,8},{10,11... | collective-permute-start | bytes 393224 | tf_op jit(solution)/shard_map/ppermute | solution.py:35
  105.3 19.2 %collective-permute-start.16 = (bf16[32,2048]{1,0:T(8,128)(2,1)S(1)}, bf16[32,2048]{1,0:T(8,128)(2,1)S(1)}, u32[]{:S(2)}, u32[]{:S(2)}) collective-permute-start(bf16[32,2048]{1,0:T(8,128)(2,1)S(1)} %collective-permute-done.8.refs_3_), channel_id=1, source_target_pairs={{0,1},{1,0},{2,3},{3,2},{4,5},{5,4},{6,7},{7,6},{8,9},{9,8},{10,11... | collective-permute-start | bytes 393224 | tf_op jit(solution)/shard_map/ppermute | solution.py:35
  107.1 22.6 %collective-permute-start.18 = (bf16[32,2048]{1,0:T(8,128)(2,1)}, bf16[32,2048]{1,0:T(8,128)(2,1)}, u32[]{:S(2)}, u32[]{:S(2)}) collective-permute-start(bf16[32,2048]{1,0:T(8,128)(2,1)} %collective-permute-done.10.refs_5_), channel_id=1, source_target_pairs={{0,1},{1,0},{2,3},{3,2},{4,5},{5,4},{6,7},{7,6},{8,9},{9,8},{10,11... | collective-permute-start | bytes 393224 | tf_op jit(solution)/shard_map/ppermute | solution.py:35
  124.5 5.2 %collective-permute-start.20 = (bf16[32,2048]{1,0:T(8,128)(2,1)}, bf16[32,2048]{1,0:T(8,128)(2,1)}, u32[]{:S(2)}, u32[]{:S(2)}) collective-permute-start(bf16[32,2048]{1,0:T(8,128)(2,1)} %collective-permute-done.12.refs_7_), channel_id=1, source_target_pairs={{0,1},{1,0},{2,3},{3,2},{4,5},{5,4},{6,7},{7,6},{8,9},{9,8},{10,11... | collective-permute-start | bytes 393224 | tf_op jit(solution)/shard_map/ppermute | solution.py:35
  125.1 20.9 %collective-permute-start.28 = (bf16[128,640]{1,0:T(8,128)(2,1)}, bf16[128,640]{1,0:T(8,128)(2,1)}, u32[]{:S(2)}, u32[]{:S(2)}) collective-permute-start(bf16[128,640]{1,0:T(8,128)(2,1)} %collective-permute-done.27.refs_2_), channel_id=1, source_target_pairs={{0,16},{16,0},{1,17},{17,1},{2,18},{18,2},{3,19},{19,3},{4,20},{20... | collective-permute-start | bytes 491528 | tf_op jit(solution)/shard_map/ppermute | solution.py:25
  148.6 1.6 collective-permute-start.29
  148.9 2.0 %collective-permute-start.32 = (bf16[64,2048]{1,0:T(8,128)(2,1)S(1)}, bf16[64,2048]{1,0:T(8,128)(2,1)S(1)}, u32[]{:S(2)}, u32[]{:S(2)}) collective-permute-start(bf16[64,2048]{1,0:T(8,128)(2,1)S(1)} %get-tuple-element.36), channel_id=1, source_target_pairs={{0,1},{1,0},{2,3},{3,2},{4,5},{5,4},{6,7},{7,6},{8,9},{9,8},{10,11... | collective-permute-start | bytes 786440 | tf_op jit(solution)/shard_map/ppermute | solution.py:35
  149.2 3.4 %collective-permute-start.35 = (bf16[64,2048]{1,0:T(8,128)(2,1)S(1)}, bf16[64,2048]{1,0:T(8,128)(2,1)S(1)}, u32[]{:S(2)}, u32[]{:S(2)}) collective-permute-start(bf16[64,2048]{1,0:T(8,128)(2,1)S(1)} %get-tuple-element.38), channel_id=1, source_target_pairs={{0,1},{1,0},{2,3},{3,2},{4,5},{5,4},{6,7},{7,6},{8,9},{9,8},{10,11... | collective-permute-start | bytes 786440 | tf_op jit(solution)/shard_map/ppermute | solution.py:35
  149.4 3.8 %collective-permute-start.38 = (bf16[64,2048]{1,0:T(8,128)(2,1)S(1)}, bf16[64,2048]{1,0:T(8,128)(2,1)S(1)}, u32[]{:S(2)}, u32[]{:S(2)}) collective-permute-start(bf16[64,2048]{1,0:T(8,128)(2,1)S(1)} %get-tuple-element.40), channel_id=1, source_target_pairs={{0,1},{1,0},{2,3},{3,2},{4,5},{5,4},{6,7},{7,6},{8,9},{9,8},{10,11... | collective-permute-start | bytes 786440 | tf_op jit(solution)/shard_map/ppermute | solution.py:35
  150.3 6.4 %collective-permute-start.30 = (bf16[1,32,2048]{2,1,0:T(8,128)(2,1)S(1)}, bf16[1,32,2048]{2,1,0:T(8,128)(2,1)S(1)}, u32[]{:S(2)}, u32[]{:S(2)}) collective-permute-start(bf16[1,32,2048]{2,1,0:T(8,128)(2,1)S(1)} %fusion.24), channel_id=1, source_target_pairs={{0,2},{1,3},{2,0},{3,1},{4,6},{5,7},{6,4},{7,5},{8,10},{9,11},{10,... | collective-permute-start | bytes 393224 | tf_op jit(solution)/shard_map/ppermute | solution.py:35
  151.0 8.5 %collective-permute-start.33 = (bf16[1,32,2048]{2,1,0:T(8,128)(2,1)S(1)}, bf16[1,32,2048]{2,1,0:T(8,128)(2,1)S(1)}, u32[]{:S(2)}, u32[]{:S(2)}) collective-permute-start(bf16[1,32,2048]{2,1,0:T(8,128)(2,1)S(1)} %fusion.26), channel_id=1, source_target_pairs={{0,2},{1,3},{2,0},{3,1},{4,6},{5,7},{6,4},{7,5},{8,10},{9,11},{10,... | collective-permute-start | bytes 393224 | tf_op jit(solution)/shard_map/ppermute | solution.py:35
  152.6 9.7 %collective-permute-start.36 = (bf16[1,32,2048]{2,1,0:T(8,128)(2,1)S(1)}, bf16[1,32,2048]{2,1,0:T(8,128)(2,1)S(1)}, u32[]{:S(2)}, u32[]{:S(2)}) collective-permute-start(bf16[1,32,2048]{2,1,0:T(8,128)(2,1)S(1)} %fusion.28), channel_id=1, source_target_pairs={{0,2},{1,3},{2,0},{3,1},{4,6},{5,7},{6,4},{7,5},{8,10},{9,11},{10,... | collective-permute-start | bytes 393224 | tf_op jit(solution)/shard_map/ppermute | solution.py:35
  153.3 11.1 %collective-permute-start.39 = (bf16[1,32,2048]{2,1,0:T(8,128)(2,1)S(1)}, bf16[1,32,2048]{2,1,0:T(8,128)(2,1)S(1)}, u32[]{:S(2)}, u32[]{:S(2)}) collective-permute-start(bf16[1,32,2048]{2,1,0:T(8,128)(2,1)S(1)} %fusion.29), channel_id=1, source_target_pairs={{0,2},{1,3},{2,0},{3,1},{4,6},{5,7},{6,4},{7,5},{8,10},{9,11},{10,... | collective-permute-start | bytes 393224 | tf_op jit(solution)/shard_map/ppermute | solution.py:35
  156.8 12.8 %copy-start.33 = (bf16[32,2048]{1,0:T(8,128)(2,1)S(1)}, bf16[32,2048]{1,0:T(8,128)(2,1)}, u32[]{:S(2)}) copy-start(bf16[32,2048]{1,0:T(8,128)(2,1)} %copy-done.32) | copy-start | bytes 393220
  156.8 12.8 %copy-start.35 = (f32[2048]{0:T(1024)S(1)}, f32[2048]{0:T(1024)}, u32[]{:S(2)}) copy-start(f32[2048]{0:T(1024)} %param.20) | copy-start | bytes 24580
  156.8 8.7 %collective-permute-start.31 = (bf16[32,2048]{1,0:T(8,128)(2,1)S(1)}, bf16[32,2048]{1,0:T(8,128)(2,1)S(1)}, u32[]{:S(2)}, u32[]{:S(2)}) collective-permute-start(bf16[32,2048]{1,0:T(8,128)(2,1)S(1)} %fusion.23), channel_id=1, source_target_pairs={{0,8},{4,12},{8,0},{12,4},{1,9},{5,13},{9,1},{13,5},{2,10},{6,14},... | collective-permute-start | bytes 393224 | tf_op jit(solution)/shard_map/ppermute | solution.py:25
  159.6 7.7 %collective-permute-start.34 = (bf16[32,2048]{1,0:T(8,128)(2,1)S(1)}, bf16[32,2048]{1,0:T(8,128)(2,1)S(1)}, u32[]{:S(2)}, u32[]{:S(2)}) collective-permute-start(bf16[32,2048]{1,0:T(8,128)(2,1)S(1)} %fusion.25), channel_id=1, source_target_pairs={{0,12},{4,0},{8,4},{12,8},{1,13},{5,1},{9,5},{13,9},{2,14},{6,2},{... | collective-permute-start | bytes 393224 | tf_op jit(solution)/shard_map/ppermute | solution.py:25
  162.4 6.9 %collective-permute-start.37 = (bf16[32,2048]{1,0:T(8,128)(2,1)S(1)}, bf16[32,2048]{1,0:T(8,128)(2,1)S(1)}, u32[]{:S(2)}, u32[]{:S(2)}) collective-permute-start(bf16[32,2048]{1,0:T(8,128)(2,1)S(1)} %fusion.27), channel_id=1, source_target_pairs={{0,4},{4,8},{8,12},{12,0},{1,5},{5,9},{9,13},{13,1},{2,6},{6,10},{... | collective-permute-start | bytes 393224 | tf_op jit(solution)/shard_map/ppermute | solution.py:25
  169.7 5.0 %collective-permute-start.41 = (bf16[32,2048]{1,0:T(8,128)(2,1)S(1)}, bf16[32,2048]{1,0:T(8,128)(2,1)S(1)}, u32[]{:S(2)}, u32[]{:S(2)}) collective-permute-start(bf16[32,2048]{1,0:T(8,128)(2,1)S(1)} %get-tuple-element.42), channel_id=1, source_target_pairs={{0,2},{1,3},{2,0},{3,1},{4,6},{5,7},{6,4},{7,5},{8,10},{9,11},{10,... | collective-permute-start | bytes 393224 | tf_op jit(solution)/shard_map/ppermute | solution.py:35
  170.3 4.4 %collective-permute-start.40 = (bf16[32,2048]{1,0:T(8,128)(2,1)S(1)}, bf16[32,2048]{1,0:T(8,128)(2,1)S(1)}, u32[]{:S(2)}, u32[]{:S(2)}) collective-permute-start(bf16[32,2048]{1,0:T(8,128)(2,1)S(1)} %get-tuple-element.42), channel_id=1, source_target_pairs={{0,1},{1,0},{2,3},{3,2},{4,5},{5,4},{6,7},{7,6},{8,9},{9,8},{10,11... | collective-permute-start | bytes 393224 | tf_op jit(solution)/shard_map/ppermute | solution.py:35
  174.8 1.3 collective-permute-start.42
  (33 other events, 39.4 us)
